TPU v7x, 128 devices: a whole 4x4x4 slice. The times are simulated.
128 devices in a mesh: sp: 32 (over z, y, core), tp: 4 (over x).
Axes of the slice: x: 4, y: 4, z: 4, core: 2. Of those that a mesh axis runs over, the one named last changes fastest.
Arguments:
- tokens: bfloat16 [16384, 2048], P(('sp', 'tp')), may hold values from -6 to 6
- queries: bfloat16 [16384, 1024], P('sp', 'tp'), may hold values from -160 to 160
- keys: bfloat16 [16384, 1024], P('sp', 'tp'), may hold values from -8 to 8
- values: bfloat16 [16384, 1024], P('sp', 'tp'), may hold values from -6 to 6
- lambdas: float32 [8], P('tp'), may hold values from 0.3 to 0.8
- head_gain: float32 [128], replicated, may hold values from 0.1 to 1.9
- out_weight: bfloat16 [1024, 2048], replicated, may hold values from -0.1875 to 0.1875
- mixer_gain: float32 [2048], replicated, may hold values from 0.1 to 1.9
- up_weight: bfloat16 [2048, 4096], P('sp', 'tp'), may hold values from -0.125 to 0.125
- down_weight: bfloat16 [4096, 2048], P('tp', 'sp'), may hold values from -0.09375 to 0.09375
Outputs:
- result: bfloat16 [16384, 2048], P(('sp', 'tp'))
All inputs are finite; a program needn't handle non-finite values.
Results may differ from a plain program's by a relative error of at most 0.02.
Values may be sent and summed in bfloat16 or wider, within the bound.
No kernel may reach another device: no remote copies, remote signals or barrier semaphores. Data moves between devices by JAX's collectives and lax.ppermute only.
A program may use at most 128 MiB of HBM per device.

v0:
```python
import functools

import jax
import jax.numpy as jnp
from jax import lax
from jax.experimental import pallas as pl
from jax.experimental.pallas import tpu as pltpu
from jax.sharding import Mesh, PartitionSpec as P


DQK = 64
DV = 128
HALF = 512
TILE = 256
BF16 = jnp.bfloat16
F32 = jnp.float32
NEG = -1e30
SEQ = ("z", "y", "c")


ROWS = DV + 16


def attend_kernel(spans, edge, last, ids_ref, lam_ref, q_ref, gain_ref, *refs):
    first = edge == "own"
    if not first:
        top_in, acc_in, *refs = refs
    pieces, refs = refs[: len(spans)], refs[len(spans) :]
    if last:
        low_ref, high_ref, tops, acc, *refs = refs
    else:
        tops, acc, *refs = refs
    held, sems, items, scores_a, scores_b, peaks_a, peaks_b = refs
    own = ids_ref[0]
    slots = held.shape[0]
    slot = 0
    for piece, span in zip(pieces, spans):
        for j in range(span):
            pltpu.make_async_copy(piece.at[j], held.at[slot], sems.at[slot]).start()
            slot += 1
    if first:
        tops[...] = jnp.full(tops.shape, NEG, F32)
        acc[...] = jnp.zeros(acc.shape, F32)
    else:
        tops[...] = top_in[...]
        acc[...] = acc_in[...]

    for slot in range(slots):
        pltpu.make_async_copy(held.at[slot], held.at[slot], sems.at[slot]).wait()

    units = [(t, m) for t in range(HALF // TILE) for m in range(2)]
    parts = 2 * HALF // TILE
    ones = jnp.ones((ROWS - DV, TILE), BF16)

    def columns(side, t):
        return pl.ds(pl.multiple_of(side * HALF, HALF) + t * TILE, TILE)

    def key_part(slot, j):
        return held[slot, j // 2, 2 * (j % 2) : 2 * (j % 2) + 2].reshape(TILE, DV)

    def value_part(slot, j):
        n = 4 + 2 * (j % 2)
        vals = jnp.concatenate([held[slot, j // 2, n], held[slot, j // 2, n + 1]], axis=1)
        return jnp.concatenate([vals, ones], axis=0)

    def score_steps(item, scores, peaks):
        slot, side = item // 2, item % 2
        for u, (t, m) in enumerate(units):
            peak = None
            for j in range(parts):
                s = jnp.dot(
                    key_part(slot, j), q_ref[m, :, columns(side, t)], preferred_element_type=F32
                )
                scores[u, j * TILE : (j + 1) * TILE, :] = s
                high = jnp.max(s.reshape(TILE // 8, 8, TILE), axis=0)
                peak = high if peak is None else jnp.maximum(peak, high)
                if j == parts - 1:
                    peaks[u] = peak
                yield

    def weight_steps(item, scores, peaks):
        slot, side = item // 2, item % 2
        for u, (t, m) in enumerate(units):
            cols = columns(side, t)
            old = tops[m, 0:1, cols]
            top = jnp.maximum(old, jnp.max(peaks[u], axis=0, keepdims=True))
            shrink = jnp.exp(old - top)
            tops[m, 0:1, cols] = top
            total = None
            for j in range(parts):
                p = jnp.exp(scores[u, j * TILE : (j + 1) * TILE, :] - top).astype(BF16)
                part = jnp.dot(value_part(slot, j), p, preferred_element_type=F32)
                total = part if total is None else total + part
                if j == parts - 1:
                    acc[m, :, cols] = acc[m, :, cols] * shrink + total
                yield

    def together(*steps):
        steps = list(steps)
        while steps:
            steps = [s for s in steps if next(s, True) is None]

    def listed(i, count):
        for side, limit in ((0, own), (1, 15 - own)):
            items[count] = 2 * i + side
            count = count + (ids_ref[1 + i] < limit).astype(jnp.int32)
        return count

    def pair(k, carry):
        one, two, three = items[2 * k], items[2 * k + 1], items[2 * k + 2]
        together(score_steps(two, scores_b, peaks_b), weight_steps(one, scores_a, peaks_a))

        @pl.when(2 * k + 1 < count)
        def _():
            together(score_steps(three, scores_a, peaks_a), weight_steps(two, scores_b, peaks_b))

        return carry

    if not first:
        count = lax.fori_loop(0, slots, listed, jnp.int32(0))
        items[count] = 0
        items[count + 1] = 0

        @pl.when(count > 0)
        def _():
            together(score_steps(items[0], scores_a, peaks_a))

        lax.fori_loop(0, (count + 1) // 2, pair, 0)

    def edge_item(slot, side, allowed):
        def tile(t, carry):
            cols = pl.ds(pl.multiple_of(side * HALF + t * TILE, TILE), TILE)
            for m in range(2):
                for j in range(parts):
                    s = jnp.dot(key_part(slot, j), q_ref[m, :, cols], preferred_element_type=F32)
                    key_pos = lax.broadcasted_iota(jnp.int32, (TILE, TILE), 0) + j * TILE
                    query_pos = lax.broadcasted_iota(jnp.int32, (TILE, TILE), 1)
                    scores_a[m, j * TILE : (j + 1) * TILE, :] = jnp.where(
                        key_pos <= query_pos + (t * TILE + allowed), s, -jnp.inf
                    )
            for m in range(2):
                old = tops[m, 0:1, cols]
                top = jnp.maximum(old, jnp.max(scores_a[m], axis=0, keepdims=True))
                shrink = jnp.exp(old - top)
                tops[m, 0:1, cols] = top
                total = None
                for j in range(parts):
                    p = jnp.exp(scores_a[m, j * TILE : (j + 1) * TILE, :] - top).astype(BF16)
                    part = jnp.dot(value_part(slot, j), p, preferred_element_type=F32)
                    total = part if total is None else total + part
                acc[m, :, cols] = acc[m, :, cols] * shrink + total
            return carry

        lax.fori_loop(0, HALF // TILE, tile, 0)

    if edge == "own":
        edge_item(0, 0, 0)

        @pl.when(own < 15 - own)
        def _():
            edge_item(0, 1, 2 * HALF)

    if edge == "other":

        def edges(i, carry):
            @pl.when(ids_ref[1 + i] == 15 - own)
            def _():
                edge_item(i, 1, HALF)

            return carry

        lax.fori_loop(0, slots, edges, 0)

    if last:
        for t in range(2 * HALF // TILE):
            cols = slice(t * TILE, (t + 1) * TILE)
            differ = acc[0, :DV, cols] / acc[0, DV : DV + 1, cols] - lam_ref[0] * (
                acc[1, :DV, cols] / acc[1, DV : DV + 1, cols]
            )
            spread = lax.rsqrt(jnp.mean(differ * differ, axis=0, keepdims=True) + 1e-06)
            out_ref = low_ref if t * TILE < HALF else high_ref
            rows = slice(t * TILE % HALF, t * TILE % HALF + TILE)
            out_ref[rows, :] = (differ * spread * gain_ref[...]).T.astype(BF16)


def attend(slots, ids, lam, query, gain, state, edge, last):
    pieces = [p if p.ndim == 5 else p[None] for p in slots]
    spans = tuple(p.shape[0] for p in pieces)
    count = sum(spans)
    vmem = pl.BlockSpec(memory_space=pltpu.VMEM)
    smem = pl.BlockSpec(memory_space=pltpu.SMEM)
    held = [
        pltpu.VMEM((count, 2, 8, DV, DV), BF16),
        pltpu.SemaphoreType.DMA((count,)),
        pltpu.SMEM((2 * count + 2,), jnp.int32),
        pltpu.VMEM((4, 2 * HALF, TILE), F32),
        pltpu.VMEM((4, 2 * HALF, TILE), F32),
        pltpu.VMEM((4, 8, TILE), F32),
        pltpu.VMEM((4, 8, TILE), F32),
    ]
    shapes = [(2, 8, 2 * HALF), (2, ROWS, 2 * HALF)]
    if last:
        out_shape = (jax.ShapeDtypeStruct((HALF, DV), BF16),) * 2
        scratch = [pltpu.VMEM(s, F32) for s in shapes] + held
        out_specs = (vmem, vmem)
    else:
        out_shape = tuple(jax.ShapeDtypeStruct(s, F32) for s in shapes)
        scratch = held
        out_specs = (vmem, vmem)
    state = [] if state is None else list(state)
    flops = count * 2 * HALF * HALF * 2 * 2 * 2 * (DV + DV) // 2
    return pl.pallas_call(
        functools.partial(attend_kernel, spans, edge, last),
        out_shape=out_shape,
        in_specs=[smem, smem, vmem, vmem]
        + [vmem] * len(state)
        + [pl.BlockSpec(memory_space=pl.ANY)] * len(pieces),
        out_specs=out_specs,
        scratch_shapes=scratch,
        cost_estimate=pl.CostEstimate(
            flops=flops, bytes_accessed=count * 2**19, transcendentals=count * 2**20
        ),
        name="attend",
    )(ids, lam, query, gain, *state, *pieces)


def square_relu(x):
    x = jnp.maximum(x, 0.0)
    return (x * x).astype(BF16)


CUTS = 8


def token_kernel(steps, x_ref, chips_ref, gain_ref, *refs):
    tokens_refs, refs = refs[: len(steps)], refs[len(steps) :]
    heads_refs, proj_ref, refs = refs[:5], refs[5], refs[6:]
    weight_refs, refs = refs[:10], refs[10:]
    outs, (heads, tokens, proj, up, down, sems) = refs[:-6], refs[-6:]
    x = x_ref[0]

    def copied(source, target, n):
        pltpu.make_async_copy(source, target, sems.at[n]).start()

    def settled(target, n):
        pltpu.make_async_copy(target, target, sems.at[n]).wait()

    for g, step in enumerate(steps):
        who = (x + step) % 4
        rows = pl.ds(pl.multiple_of(who * 128, 128), 128)
        here = pl.ds(g * 128, 128)
        copied(tokens_refs[g], tokens.at[here], 1)
        for back, source in zip((0, 3, 1), heads_refs):
            cols = pl.ds(pl.multiple_of((x + back) % 4 * 256, 256), 256)
            copied(source.at[rows], heads.at[here, cols], 0)
        cols = pl.ds(pl.multiple_of((x + 2) % 4 * 256, 256), 256)
        half = pl.ds(pl.multiple_of(who % 2 * 128, 128), 128)

        @pl.when(who < 2)
        def _(half=half, here=here, cols=cols):
            copied(heads_refs[3].at[half], heads.at[here, cols], 0)

        @pl.when(who >= 2)
        def _(half=half, here=here, cols=cols):
            copied(heads_refs[4].at[half], heads.at[here, cols], 0)

    for n in range(CUTS):
        part = pl.ds(n * 1024 // CUTS, 1024 // CUTS)
        copied(proj_ref.at[part], proj.at[part], 2)
    for kind, target in enumerate((up, down)):
        for half in range(2):
            slot = 0
            for piece in weight_refs[5 * half : 5 * half + 5]:
                for j in range(piece.shape[0]):
                    copied(
                        piece.at[j, kind], target.at[half, chips_ref[16 * half + slot]], 3 + kind
                    )
                    slot += 1

    settled(heads, 0)
    settled(tokens, 1)
    settled(proj, 2)
    projected = jnp.dot(heads[...], proj[...], preferred_element_type=F32).astype(BF16)
    resid = (tokens[...].astype(F32) + projected.astype(F32)).astype(BF16)
    wide = resid.astype(F32)
    spread = lax.rsqrt(jnp.mean(wide * wide, axis=1, keepdims=True) + 1e-06)
    tokens[...] = resid
    normed = (wide * spread * gain_ref[...]).astype(BF16)
    settled(up, 3)
    made = [
        square_relu(
            jnp.dot(normed, up[half].reshape(2048, 512), preferred_element_type=F32)
        )
        for half in range(2)
    ]
    settled(down, 4)
    for n in range(0, 2048, 512):
        cols = slice(n, n + 512)
        part = None
        for half in range(2):
            term = lax.dot_general(
                made[half],
                down[half, n // 128 : n // 128 + 4].reshape(512, 512),
                (((1,), (1,)), ((), ())),
                preferred_element_type=F32,
            )
            part = term if part is None else part + term
        if steps == (0,):
            outs[0][:, cols] = part + tokens[:, cols].astype(F32)
        else:
            size = outs[0].shape[0]
            for g, out in enumerate(outs):
                out[:, cols] = part[g * size : (g + 1) * size].astype(BF16)


def token_parts(steps, x, chips, gain, tokens, parts):
    count = len(steps)
    pieces = 1 if steps == (0,) else 2
    kind = F32 if steps == (0,) else BF16
    vmem = pl.BlockSpec(memory_space=pltpu.VMEM)
    smem = pl.BlockSpec(memory_space=pltpu.SMEM)
    return pl.pallas_call(
        functools.partial(token_kernel, steps),
        out_shape=[jax.ShapeDtypeStruct((count * 128 // pieces, 2048), kind)] * pieces,
        in_specs=[smem, smem, vmem]
        + [pl.BlockSpec(memory_space=pl.ANY)] * (count + len(parts)),
        out_specs=[vmem] * pieces,
        scratch_shapes=[
            pltpu.VMEM((count * 128, 1024), BF16),
            pltpu.VMEM((count * 128, 2048), BF16),
            pltpu.VMEM((1024, 2048), BF16),
            pltpu.VMEM((2, 16, 128, 512), BF16),
            pltpu.VMEM((2, 16, 128, 512), BF16),
            pltpu.SemaphoreType.DMA((5,)),
        ],
        cost_estimate=pl.CostEstimate(
            flops=count * 128 * 2048 * 3072 * 2, bytes_accessed=12 * 2**20, transcendentals=0
        ),
        name="token_parts",
    )(x, chips, gain, *tokens, *parts)


def ring_pairs(axis, step):
    pairs = []
    for z in range(4):
        for y in range(4):
            for core in range(2):
                if (axis == 1) == (core == 0):
                    to = z * 4 + (y + step) % 4
                else:
                    to = (z + step) % 4 * 4 + y
                pairs.append(((z * 4 + y) * 2 + core, to * 2 + core))
    return pairs


PAIRS = {(axis, step): ring_pairs(axis, step) for axis in (1, 2) for step in (1, -1)}


def passed(array, axis, step):
    return lax.ppermute(array, SEQ, PAIRS[axis, step])


def source_chip(a, b, core=0):
    z, y = lax.axis_index("z"), lax.axis_index("y")
    first = lax.axis_index("c") == core
    dz, dy = jnp.where(first, b, a), jnp.where(first, a, b)
    return (z + dz + 4) % 4 * 4 + (y + dy + 4) % 4


def per_device(
    tokens,
    queries,
    keys,
    values,
    lambdas,
    head_gain,
    out_weight,
    mixer_gain,
    up_weight,
    down_weight,
):
    core = lax.axis_index("c")
    chip = lax.axis_index("z") * 4 + lax.axis_index("y")
    first = core == 0
    swap = [(0, 1), (1, 0)]

    def along_x(array, step):
        return lax.ppermute(array, "x", [(i, (i + step) % 4) for i in range(4)])

    def swapped(array):
        return lax.ppermute(array, "c", swap)

    scaled = queries * jnp.asarray(DQK ** (-0.5), BF16)

    def packed(head):
        cols = slice(head * DV, (head + 1) * DV)
        k = keys[:, cols].reshape(4, DV, DV)
        v = values[:, cols].reshape(4, DV, DV)
        q = scaled[:, cols].reshape(4, DV, DV)
        return jnp.concatenate([k, jnp.swapaxes(v, 1, 2), q], axis=0)

    head_a, head_b = packed(0), packed(1)
    keep = jnp.where(first, head_a, head_b)
    other = swapped(jnp.where(first, head_b, head_a))
    even, odd = jnp.where(first, keep, other), jnp.where(first, other, keep)
    chunk = jnp.stack([even[:8], odd[:8]])

    def flat(chip_id, core_id):
        return chip_id * 2 + core_id

    high = lax.ppermute(odd[8:], ("z", "y"), [(i, 15 - i) for i in range(16)])
    query = jnp.concatenate([even[8:].reshape(HALF, DV), high.reshape(HALF, DV)], axis=0).T
    none = jnp.zeros((DQK, 2 * HALF), BF16)
    query = jnp.stack(
        [
            jnp.concatenate([query[:DQK], none], axis=0),
            jnp.concatenate([none, query[DQK:]], axis=0),
        ]
    )

    lam = jnp.where(first, lambdas[0:1], lambdas[1:2])
    gain = head_gain[:, None]

    def attending(slots, state, edge=None, last=False):
        places = [p for place, _ in slots for p in (place if isinstance(place[0], tuple) else (place,))]
        ids = jnp.stack([chip] + [source_chip(*place) for place in places])
        return attend([c for _, c in slots], ids, lam, query, gain, state, edge, last)

    near_p, near_n = passed(chunk, 1, 1), passed(chunk, 1, -1)
    state = attending([((0, 0), chunk)], None, "own")
    across = passed(near_p, 1, 1)
    pair_a = jnp.stack([chunk, near_p])
    a_p, a_n = passed(pair_a, 2, 1), passed(pair_a, 2, -1)
    pair_b = jnp.stack([near_n, across])
    b_p, b_n = passed(pair_b, 2, 1), passed(pair_b, 2, -1)
    over_p = passed(a_p, 2, 1)
    state = attending(
        [
            ((-1, 0), near_p),
            ((1, 0), near_n),
            ((2, 0), across),
            (((0, -1), (-1, -1)), a_p),
            (((0, 1), (-1, 1)), a_n),
        ],
        state,
        "other",
    )
    over_n = passed(b_n, 2, -1)
    state = attending([(((1, -1), (2, -1)), b_p), (((1, 1), (2, 1)), b_n)], state, "other")

    tokens_p, tokens_n = along_x(tokens, 1), along_x(tokens, -1)
    tokens_far = along_x(tokens_p, 1)
    both = jnp.stack([up_weight, down_weight.T])
    both_a, both_b = both[:, :, :512], both[:, :, 512:]
    keep = jnp.where(first, both_a, both_b)
    other = swapped(jnp.where(first, both_b, both_a))
    unit = jnp.concatenate(
        [jnp.where(first, keep, other), jnp.where(first, other, keep)], axis=1
    )
    unit_p, unit_n = passed(unit, 1, 1), passed(unit, 1, -1)
    unit_f = passed(unit_p, 1, 1)
    row = jnp.stack([unit, unit_p, unit_n, unit_f])
    row_p, row_n = passed(row, 2, 1), passed(row, 2, -1)
    row_a, row_b = passed(row_p[:2], 2, 1), passed(row_n[2:], 2, -1)
    weights = [row, row_p, row_n, row_a, row_b]
    weights += [swapped(w) for w in weights]
    near = (0, -1, 1, 2)
    chips = jnp.stack(
        [
            source_chip(a, b, core)
            for core in (0, 1)
            for places in ((near, 0), (near, -1), (near, 1), (near, 2))
            for a, b in ((n, places[1]) for n in places[0])
        ]
    )
    low, high = attending(
        [(((0, 2), (-1, 2)), over_p), (((1, 2), (2, 2)), over_n)], state, last=True
    )

    back = [(flat(i, 1), flat(i, 0)) for i in range(16)] + [
        (flat(i, 0), flat(15 - i, 1)) for i in range(16)
    ]
    flip = [(flat(i, 1), flat(15 - i, 1)) for i in range(16)]
    got_far = lax.ppermute(high, SEQ, flip)
    got = lax.ppermute(jnp.where(first, high, low), SEQ, back)
    attended = jnp.concatenate([jnp.where(first, low, got), jnp.where(first, got, got_far)], axis=1)

    prev, following = along_x(attended, 1), along_x(attended, -1)
    far_top = along_x(prev[:256], 1)
    far_low = along_x(following[256:], -1)
    x = lax.axis_index("x")[None]
    parts = (attended, prev, following, far_top, far_low, out_weight, *weights)
    gain = mixer_gain[None]
    far_top_part, far_low_part = token_parts((2,), x, chips, gain, (tokens_far,), parts)
    from_prev = along_x(far_top_part, 1)
    from_next = along_x(far_low_part, -1)
    prev_part, next_part = token_parts((3, 1), x, chips, gain, (tokens_p, tokens_n), parts)

    def added(a, b):
        return (a.astype(F32) + b.astype(F32)).astype(BF16)

    none = jnp.zeros((64, 2048), BF16)
    to_next = added(next_part, jnp.concatenate([from_prev, none], axis=0))
    to_prev = added(prev_part, jnp.concatenate([none, from_next], axis=0))
    got_prev = along_x(to_next, 1)
    got_next = along_x(to_prev, -1)
    (total,) = token_parts((0,), x, chips, gain, (tokens,), parts)
    return (total + got_prev.astype(F32) + got_next.astype(F32)).astype(BF16)


def solution(mesh):
    grid = Mesh(mesh.devices.reshape(4, 4, 2, 4), ("z", "y", "c", "x"))
    placed = (
        P((*SEQ, "x"), None),
        P(SEQ, "x"),
        P(SEQ, "x"),
        P(SEQ, "x"),
        P("x"),
        P(),
        P(),
        P(),
        P(SEQ, "x"),
        P("x", SEQ),
    )

    return jax.shard_map(
        per_device, mesh=grid, in_specs=placed, out_specs=P((*SEQ, "x"), None), check_vma=False
    )
```

profile of v0, /device:TPU:32, one launch (start us, length us, event | category | flops | bytes accessed | tf_op | source)
XLA Modules:
  0.0 197.8 jit_solution(9255489943600104937)
XLA Ops:
  0.0 1.0 broadcast_multiply_fusion
  1.6 1.7 collective-permute-done
  3.6 1.6 collective-permute-start.2
  5.2 1.7 collective-permute-start.3
  6.9 7.2 %collective-permute-done.2 = bf16[2,8,128,128]{3,2,1,0:T(8,128)(2,1)S(1)} collective-permute-done((bf16[2,8,128,128]{3,2,1,0:T(8,128)(2,1)S(1)}, bf16[2,8,128,128]{3,2,1,0:T(8,128)(2,1)S(1)}, u32[]{:S(2)}, u32[]{:S(2)}) %collective-permute-start.2) | collective-permute-done | bytes 524320 | tf_op jit(solution)/shard_map/ppermute | solution.py:360
  14.0 0.4 collective-permute-start.4
  14.5 2.0 %collective-permute-start.5 = (bf16[2,2,8,128,128]{4,3,2,1,0:T(8,128)(2,1)S(1)}, bf16[2,2,8,128,128]{4,3,2,1,0:T(8,128)(2,1)}, u32[]{:S(2)}, u32[]{:S(2)}) collective-permute-start(bf16[2,2,8,128,128]{4,3,2,1,0:T(8,128)(2,1)S(1)} %pad_maximum_fusion), channel_id=1, source_target_pairs={{0,32},{4,12},{8,40},{12,20},{16,48},{20,28},{24,56},{28,4},{32,64... | collective-permute-start | bytes 3145736 | tf_op jit(solution)/shard_map/ppermute | solution.py:360
  16.7 13.4 %collective-permute-done.4 = bf16[2,8,128,128]{3,2,1,0:T(8,128)(2,1)S(1)} collective-permute-done((bf16[2,8,128,128]{3,2,1,0:T(8,128)(2,1)S(1)}, bf16[2,8,128,128]{3,2,1,0:T(8,128)(2,1)S(1)}, u32[]{:S(2)}, u32[]{:S(2)}) %collective-permute-start.4) | collective-permute-done | bytes 524320 | tf_op jit(solution)/shard_map/ppermute | solution.py:360
  30.1 1.2 pad_maximum_fusion.1
  31.5 3.2 %collective-permute-start.19 = (bf16[2,128,512]{2,1,0:T(8,128)(2,1)S(1)}, bf16[2,128,512]{2,1,0:T(8,128)(2,1)S(1)}, u32[]{:S(2)}, u32[]{:S(2)}) collective-permute-start(bf16[2,128,512]{2,1,0:T(8,128)(2,1)S(1)} %get-tuple-element.36), channel_id=1, source_target_pairs={{0,24},{4,100},{8,0},{12,108},{16,8},{20,116},{24,16},{28,124},{32... | collective-permute-start | bytes 786440 | tf_op jit(solution)/shard_map/ppermute | solution.py:360
  34.7 4.1 %collective-permute-start.6 = (bf16[2,2,8,128,128]{4,3,2,1,0:T(8,128)(2,1)S(1)}, bf16[2,2,8,128,128]{4,3,2,1,0:T(8,128)(2,1)}, u32[]{:S(2)}, u32[]{:S(2)}) collective-permute-start(bf16[2,2,8,128,128]{4,3,2,1,0:T(8,128)(2,1)S(1)} %pad_maximum_fusion), channel_id=1, source_target_pairs={{0,96},{4,28},{8,104},{12,4},{16,112},{20,12},{24,120},{28,20},{32... | collective-permute-start | bytes 3145736 | tf_op jit(solution)/shard_map/ppermute | solution.py:360
  38.9 0.2 collective-permute-done.18
  39.1 1.2 collective-permute-start.1
  40.2 1.2 collective-permute-done.19
  41.4 0.6 fusion.6
  42.0 4.2 %collective-permute-done.1 = bf16[4,128,128]{2,1,0:T(8,128)(2,1)S(1)} collective-permute-done((bf16[4,128,128]{2,1,0:T(8,128)(2,1)S(1)}, bf16[4,128,128]{2,1,0:T(8,128)(2,1)S(1)}, u32[]{:S(2)}, u32[]{:S(2)}) %collective-permute-start.1) | collective-permute-done | bytes 131104 | tf_op jit(solution)/shard_map/ppermute | solution.py:411
  46.3 2.0 %collective-permute-start.7 = (bf16[2,2,8,128,128]{4,3,2,1,0:T(8,128)(2,1)}, bf16[2,2,8,128,128]{4,3,2,1,0:T(8,128)(2,1)}, u32[]{:S(2)}, u32[]{:S(2)}) collective-permute-start(bf16[2,2,8,128,128]{4,3,2,1,0:T(8,128)(2,1)} %pad_maximum_fusion.1), channel_id=1, source_target_pairs={{0,32},{4,12},{8,40},{12,20},{16,48},{20,28},{24,56},{28,4},{32,64... | collective-permute-start | bytes 3145736 | tf_op jit(solution)/shard_map/ppermute | solution.py:360
  48.3 3.1 %collective-permute-start.9 = (bf16[2,2,8,128,128]{4,3,2,1,0:T(8,128)(2,1)}, bf16[2,2,8,128,128]{4,3,2,1,0:T(8,128)(2,1)}, u32[]{:S(2)}, u32[]{:S(2)}) collective-permute-start(bf16[2,2,8,128,128]{4,3,2,1,0:T(8,128)(2,1)} %collective-permute-done.5.refs_5_), channel_id=1, source_target_pairs={{0,32},{4,12},{8,40},{12,20},{16,48},{20,28},{24,56},{28,4},{32,64... | collective-permute-start | bytes 3145736 | tf_op jit(solution)/shard_map/ppermute | solution.py:360
  51.4 0.6 pad_add_fusion.ids_ref
  52.0 0.7 copy.24.gain_ref
  54.0 0.6 stack.207.ids_ref
  54.6 0.7 stack.211.ids_ref
  55.3 0.6 stack.212.ids_ref
  56.2 1.6 collective-permute-start.30
  57.8 1.5 collective-permute-start.10
  59.4 0.8 pad_maximum_fusion.3.q_ref
  60.3 6.5 %attend.4 = (f32[2,8,1024]{2,1,0:T(8,128)}, f32[2,144,1024]{2,1,0:T(8,128)}) custom-call(s32[2]{0:T(128)} %pad_add_fusion.ids_ref, f32[1]{0:T(128)S(6)} %select_n.598.lam_ref, bf16[2,128,1024]{2,1,0:T(8,128)(2,1)} %pad_maximum_fusion.3.q_ref, f32[128,1]{1,0:T(8,128)} %copy.24.gain_ref, bf16[1,2,8,128,128]{4,3,2,1,0:T(8,128)(2,1)} %copy-done.10), custom_call_target="tpu_custom_call" | custom-call | flops 536870912 | bytes 524288 | tf_op jit(solution)/shard_map/attend/pallas_call | solution.py:212
  67.0 0.4 collective-permute-done.30.refs_0_
  67.4 7.4 %collective-permute-start.21 = (bf16[4,2,128,512]{3,2,1,0:T(8,128)(2,1)S(1)}, bf16[4,2,128,512]{3,2,1,0:T(8,128)(2,1)S(1)}, u32[]{:S(2)}, u32[]{:S(2)}) collective-permute-start(bf16[4,2,128,512]{3,2,1,0:T(8,128)(2,1)S(1)} %pad_maximum_fusion.2.refs_7_.refs_8_), channel_id=1, source_target_pairs={{0,32},{4,12},{8,40},{12,20},{16,48},{20,28},{24,56},{28,4},{32,64... | collective-permute-start | bytes 3145736 | tf_op jit(solution)/shard_map/ppermute | solution.py:360
  74.9 15.8 %attend.5 = (f32[2,8,1024]{2,1,0:T(8,128)}, f32[2,144,1024]{2,1,0:T(8,128)}) custom-call(s32[8]{0:T(128)} %stack.212.ids_ref, f32[1]{0:T(128)S(6)} %select_n.598.lam_ref, bf16[2,128,1024]{2,1,0:T(8,128)(2,1)} %pad_maximum_fusion.3.q_ref, f32[128,1]{1,0:T(8,128)} %copy.24.gain_ref, f32[2,8,1024]{2,1,0:T(8,128)} %get-tuple-element.17.refs_0_, ...), custom_call_target="tpu_custom_call" | custom-call | flops 3758096384 | bytes 3670016 | tf_op jit(solution)/shard_map/attend/pallas_call | solution.py:212
  90.6 0.4 collective-permute-start.32
  91.0 2.2 %collective-permute-start.25 = (bf16[4,2,128,512]{3,2,1,0:T(8,128)(2,1)S(1)}, bf16[4,2,128,512]{3,2,1,0:T(8,128)(2,1)}, u32[]{:S(2)}, u32[]{:S(2)}) collective-permute-start(bf16[4,2,128,512]{3,2,1,0:T(8,128)(2,1)S(1)} %pad_maximum_fusion.2.refs_7_.refs_8_), channel_id=1, source_target_pairs={{0,4},{4,0},{1,5},{5,1},{2,6},{6,2},{3,7},{7,3},{8,12},{12,8},{9,1... | collective-permute-start | bytes 3145736 | tf_op jit(solution)/shard_map/ppermute | solution.py:391
  93.2 11.2 %attend.6 = (f32[2,8,1024]{2,1,0:T(8,128)}, f32[2,144,1024]{2,1,0:T(8,128)}) custom-call(s32[5]{0:T(128)} %stack.211.ids_ref, f32[1]{0:T(128)S(6)} %select_n.598.lam_ref, bf16[2,128,1024]{2,1,0:T(8,128)(2,1)} %pad_maximum_fusion.3.q_ref, f32[128,1]{1,0:T(8,128)} %copy.24.gain_ref, f32[2,8,1024]{2,1,0:T(8,128)} %get-tuple-element.19.refs_0_, ...), custom_call_target="tpu_custom_call" | custom-call | flops 2147483648 | bytes 2097152 | tf_op jit(solution)/shard_map/attend/pallas_call | solution.py:212
  104.4 4.0 %attend.7 = (bf16[512,128]{1,0:T(8,128)(2,1)}, bf16[512,128]{1,0:T(8,128)(2,1)}) custom-call(s32[5]{0:T(128)} %stack.207.ids_ref, f32[1]{0:T(128)S(6)} %select_n.598.lam_ref, bf16[2,128,1024]{2,1,0:T(8,128)(2,1)} %pad_maximum_fusion.3.q_ref, f32[128,1]{1,0:T(8,128)} %copy.24.gain_ref, f32[2,8,1024]{2,1,0:T(8,128)} %get-tuple-element.21.refs_0_, ...), custom_call_target="tpu_custom_call" | custom-call | flops 2147483648 | bytes 2097152 | tf_op jit(solution)/shard_map/attend/pallas_call | solution.py:212
  108.5 1.0 broadcast_select_fusion.10
  109.4 3.3 %collective-permute-start.11 = (bf16[512,128]{1,0:T(8,128)(2,1)S(1)}, bf16[512,128]{1,0:T(8,128)(2,1)S(1)}, u32[]{:S(2)}, u32[]{:S(2)}) collective-permute-start(bf16[512,128]{1,0:T(8,128)(2,1)S(1)} %broadcast_select_fusion.10), channel_id=1, source_target_pairs={{4,0},{12,8},{20,16},{28,24},{36,32},{44,40},{52,48},{60,56},{68,6... | collective-permute-start | bytes 393224 | tf_op jit(solution)/shard_map/ppermute | solution.py:485
  112.8 0.7 collective-permute-start.12
  113.5 5.7 %collective-permute-start.26 = (bf16[4,2,128,512]{3,2,1,0:T(8,128)(2,1)S(1)}, bf16[4,2,128,512]{3,2,1,0:T(8,128)(2,1)S(1)}, u32[]{:S(2)}, u32[]{:S(2)}) collective-permute-start(bf16[4,2,128,512]{3,2,1,0:T(8,128)(2,1)S(1)} %collective-permute-done.21.refs_8_.refs_9_), channel_id=1, source_target_pairs={{0,4},{4,0},{1,5},{5,1},{2,6},{6,2},{3,7},{7,3},{8,12},{12,8},{9,1... | collective-permute-start | bytes 3145736 | tf_op jit(solution)/shard_map/ppermute | solution.py:391
  119.4 1.1 collective-permute-start.23
  120.5 1.1 collective-permute-start.24
  121.7 1.8 collective-permute-start.13
  123.5 5.3 %collective-permute-done.23.refs_10_.refs_11_ = bf16[2,2,128,512]{3,2,1,0:T(8,128)(2,1)} collective-permute-done((bf16[2,2,128,512]{3,2,1,0:T(8,128)(2,1)S(1)}, bf16[2,2,128,512]{3,2,1,0:T(8,128)(2,1)}, u32[]{:S(2)}, u32[]{:S(2)}) %collective-permute-start.23) | collective-permute-done | bytes 524320 | tf_op jit(solution)/shard_map/ppermute | solution.py:360
  128.7 2.7 %collective-permute-start.14 = (bf16[512,256]{1,0:T(8,128)(2,1)S(1)}, bf16[512,256]{1,0:T(8,128)(2,1)S(1)}, u32[]{:S(2)}, u32[]{:S(2)}) collective-permute-start(bf16[512,256]{1,0:T(8,128)(2,1)S(1)} %pad_maximum_fusion.7.refs_1_.refs_2_), channel_id=1, source_target_pairs={{0,3},{1,0},{2,1},{3,2},{4,7},{5,4},{6,5},{7,6},{8,11},{9,8},{10,9... | collective-permute-start | bytes 786440 | tf_op jit(solution)/shard_map/ppermute | solution.py:388
  131.4 1.5 collective-permute-start.28
  133.0 4.3 %collective-permute-done.14.refs_3_.refs_4_ = bf16[512,256]{1,0:T(8,128)(2,1)S(1)} collective-permute-done((bf16[512,256]{1,0:T(8,128)(2,1)S(1)}, bf16[512,256]{1,0:T(8,128)(2,1)S(1)}, u32[]{:S(2)}, u32[]{:S(2)}) %collective-permute-start.14) | collective-permute-done | bytes 262176 | tf_op jit(solution)/shard_map/ppermute | solution.py:388
  137.3 3.7 %collective-permute-start.31 = (bf16[128,2048]{1,0:T(8,128)(2,1)}, bf16[128,2048]{1,0:T(8,128)(2,1)}, u32[]{:S(2)}, u32[]{:S(2)}) collective-permute-start(bf16[128,2048]{1,0:T(8,128)(2,1)} %refs_0_.1), channel_id=1, source_target_pairs={{0,3},{1,0},{2,1},{3,2},{4,7},{5,4},{6,5},{7,6},{8,11},{9,8},{10,9... | collective-permute-start | bytes 1572872 | tf_op jit(solution)/shard_map/ppermute | solution.py:388
  141.0 0.7 slice.85
  141.8 0.9 copy-done.3
  142.6 1.0 copy-done.4
  143.6 2.4 %collective-permute-start.16 = (bf16[256,256]{1,0:T(8,128)(2,1)S(1)}, bf16[256,256]{1,0:T(8,128)(2,1)S(1)}, u32[]{:S(2)}, u32[]{:S(2)}) collective-permute-start(bf16[256,256]{1,0:T(8,128)(2,1)S(1)} %slice.86), channel_id=1, source_target_pairs={{0,3},{1,0},{2,1},{3,2},{4,7},{5,4},{6,5},{7,6},{8,11},{9,8},{10,9... | collective-permute-start | bytes 393224 | tf_op jit(solution)/shard_map/ppermute | solution.py:388
  146.0 0.7 stack.205.chips_ref
  146.7 2.2 %collective-permute-done.15.refs_4_.refs_5_ = bf16[256,256]{1,0:T(8,128)(2,1)S(1)} collective-permute-done((bf16[256,256]{1,0:T(8,128)(2,1)}, bf16[256,256]{1,0:T(8,128)(2,1)S(1)}, u32[]{:S(2)}, u32[]{:S(2)}) %collective-permute-start.15) | collective-permute-done | bytes 131104 | tf_op jit(solution)/shard_map/ppermute | solution.py:388
  148.9 7.1 %collective-permute-done.16.refs_5_.refs_6_ = bf16[256,256]{1,0:T(8,128)(2,1)S(1)} collective-permute-done((bf16[256,256]{1,0:T(8,128)(2,1)S(1)}, bf16[256,256]{1,0:T(8,128)(2,1)S(1)}, u32[]{:S(2)}, u32[]{:S(2)}) %collective-permute-start.16) | collective-permute-done | bytes 131104 | tf_op jit(solution)/shard_map/ppermute | solution.py:388
  156.0 0.6 copy-done.12
  156.6 7.8 %token_parts.5 = (bf16[64,2048]{1,0:T(8,128)(2,1)}, bf16[64,2048]{1,0:T(8,128)(2,1)}) custom-call(s32[1]{0:T(128)} %bitcast.x_ref, s32[32]{0:T(128)} %stack.205.chips_ref, f32[1,2048]{1,0:T(1,128)} %bitcast.98, bf16[128,2048]{1,0:T(8,128)(2,1)} %collective-permute-done.32.refs_0_, bf16[512,256]{1,0:T(8,128)(2,1)} %copy-done.7, bf16[512,256]{1,0:T(8,128)(2,1)} %copy-done.8, ...), custom_call_target="tpu_custom_call" | custom-call | flops 1610612736 | bytes 12582912 | tf_op jit(solution)/shard_map/token_parts/pallas_call | solution.py:322
  164.4 3.8 %collective-permute-start.35 = (bf16[64,2048]{1,0:T(8,128)(2,1)}, bf16[64,2048]{1,0:T(8,128)(2,1)S(1)}, u32[]{:S(2)}, u32[]{:S(2)}) collective-permute-start(bf16[64,2048]{1,0:T(8,128)(2,1)} %get-tuple-element.28), channel_id=1, source_target_pairs={{0,3},{1,0},{2,1},{3,2},{4,7},{5,4},{6,5},{7,6},{8,11},{9,8},{10,9... | collective-permute-start | bytes 786440 | tf_op jit(solution)/shard_map/ppermute | solution.py:388
  168.2 8.5 %token_parts.4 = (bf16[128,2048]{1,0:T(8,128)(2,1)}, bf16[128,2048]{1,0:T(8,128)(2,1)}) custom-call(s32[1]{0:T(128)} %bitcast.x_ref, s32[32]{0:T(128)} %stack.205.chips_ref, f32[1,2048]{1,0:T(1,128)} %bitcast.99, bf16[128,2048]{1,0:T(8,128)(2,1)} %collective-permute-done.30.refs_0_, bf16[128,2048]{1,0:T(8,128)(2,1)} %collective-permute-done.31.refs_1_, ...), custom_call_target="tpu_custom_call" | custom-call | flops 3221225472 | bytes 12582912 | tf_op jit(solution)/shard_map/token_parts/pallas_call | solution.py:322
  176.7 1.2 add_convert_fusion.1
  177.9 3.3 %collective-permute-start.36 = (bf16[128,2048]{1,0:T(8,128)(2,1)S(1)}, bf16[128,2048]{1,0:T(8,128)(2,1)S(1)}, u32[]{:S(2)}, u32[]{:S(2)}) collective-permute-start(bf16[128,2048]{1,0:T(8,128)(2,1)S(1)} %add_convert_fusion.1), channel_id=1, source_target_pairs={{0,3},{1,0},{2,1},{3,2},{4,7},{5,4},{6,5},{7,6},{8,11},{9,8},{10,9... | collective-permute-start | bytes 1572872 | tf_op jit(solution)/shard_map/ppermute | solution.py:388
  181.3 0.3 collective-permute-start.34
  181.6 8.1 %token_parts.3 = f32[128,2048]{1,0:T(8,128)} custom-call(s32[1]{0:T(128)} %bitcast.x_ref, s32[32]{0:T(128)} %stack.205.chips_ref, f32[1,2048]{1,0:T(1,128)} %bitcast.100, bf16[128,2048]{1,0:T(8,128)(2,1)} %refs_0_.1, bf16[512,256]{1,0:T(8,128)(2,1)} %copy-done.7, bf16[512,256]{1,0:T(8,128)(2,1)} %copy-done.8, bf16[512,256]{1,0:T(8,128)(2,1)} %copy-done.9, ...), custom_call_target="tpu_custom_call" | custom-call | flops 1610612736 | bytes 12582912 | tf_op jit(solution)/shard_map/token_parts/pallas_call | solution.py:322
  189.7 2.0 %collective-permute-done.36 = bf16[128,2048]{1,0:T(8,128)(2,1)S(1)} collective-permute-done((bf16[128,2048]{1,0:T(8,128)(2,1)S(1)}, bf16[128,2048]{1,0:T(8,128)(2,1)S(1)}, u32[]{:S(2)}, u32[]{:S(2)}) %collective-permute-start.36) | collective-permute-done | bytes 524320 | tf_op jit(solution)/shard_map/ppermute | solution.py:388
  191.7 3.8 %collective-permute-done.34 = bf16[128,2048]{1,0:T(8,128)(2,1)S(1)} collective-permute-done((bf16[128,2048]{1,0:T(8,128)(2,1)S(1)}, bf16[128,2048]{1,0:T(8,128)(2,1)S(1)}, u32[]{:S(2)}, u32[]{:S(2)}) %collective-permute-start.34) | collective-permute-done | bytes 524320 | tf_op jit(solution)/shard_map/ppermute | solution.py:388
  195.6 2.2 %add_convert_fusion = bf16[128,2048]{1,0:T(8,128)(2,1)} fusion(bf16[128,2048]{1,0:T(8,128)(2,1)S(1)} %collective-permute-done.36, f32[128,2048]{1,0:T(8,128)} %token_parts.3, bf16[128,2048]{1,0:T(8,128)(2,1)S(1)} %collective-permute-done.34), kind=kLoop, calls=%fused_computation.3 | loop fusion | flops 1310720 | bytes 2621440 | tf_op jit(solution)/shard_map/convert_element_type | solution.py:508
  (108 shorter events, 2.3 us)
Async XLA Ops:
  0.0 1.1 copy-start.20
  0.0 1.2 copy-start.21
  1.5 1.8 collective-permute-start
  3.5 13.0 %copy-start.10 = (bf16[1,2,8,128,128]{4,3,2,1,0:T(8,128)(2,1)}, bf16[1,2,8,128,128]{4,3,2,1,0:T(8,128)(2,1)S(1)}, u32[]{:S(2)}) copy-start(bf16[1,2,8,128,128]{4,3,2,1,0:T(8,128)(2,1)S(1)} %get-tuple-element.32.refs_0_) | copy-start | bytes 1572868
  3.6 12.9 %copy-start.14 = (bf16[1024,64]{0,1:T(8,128)(2,1)S(1)}, bf16[1024,64]{0,1:T(8,128)(2,1)}, u32[]{:S(2)}) copy-start(bf16[1024,64]{0,1:T(8,128)(2,1)} %param.19) | copy-start | bytes 393220
  3.6 12.9 %copy-start.15 = (bf16[64,1024]{1,0:T(8,128)(2,1)S(1)}, bf16[64,1024]{1,0:T(8,128)(2,1)}, u32[]{:S(2)}) copy-start(bf16[64,1024]{1,0:T(8,128)(2,1)} %param.18) | copy-start | bytes 393220
  3.6 10.5 %collective-permute-start.2 = (bf16[2,8,128,128]{3,2,1,0:T(8,128)(2,1)S(1)}, bf16[2,8,128,128]{3,2,1,0:T(8,128)(2,1)S(1)}, u32[]{:S(2)}, u32[]{:S(2)}) collective-permute-start(bf16[2,8,128,128]{3,2,1,0:T(8,128)(2,1)S(1)} %get-tuple-element.31), channel_id=1, source_target_pairs={{0,8},{4,36},{8,16},{12,44},{16,24},{20,52},{24,0},{28,60},{32,40}... | collective-permute-start | bytes 1572872 | tf_op jit(solution)/shard_map/ppermute | solution.py:360
  5.2 11.4 %collective-permute-start.3 = (bf16[2,8,128,128]{3,2,1,0:T(8,128)(2,1)S(1)}, bf16[2,8,128,128]{3,2,1,0:T(8,128)(2,1)S(1)}, u32[]{:S(2)}, u32[]{:S(2)}) collective-permute-start(bf16[2,8,128,128]{3,2,1,0:T(8,128)(2,1)S(1)} %get-tuple-element.31), channel_id=1, source_target_pairs={{0,24},{4,100},{8,0},{12,108},{16,8},{20,116},{24,16},{28,124},{32... | collective-permute-start | bytes 1572872 | tf_op jit(solution)/shard_map/ppermute | solution.py:360
  14.0 2.5 %copy-start.17 = (bf16[2,8,128,128]{3,2,1,0:T(8,128)(2,1)}, bf16[2,8,128,128]{3,2,1,0:T(8,128)(2,1)S(1)}, u32[]{:S(2)}) copy-start(bf16[2,8,128,128]{3,2,1,0:T(8,128)(2,1)S(1)} %collective-permute-done.2) | copy-start | bytes 1572868
  14.0 16.0 %collective-permute-start.4 = (bf16[2,8,128,128]{3,2,1,0:T(8,128)(2,1)S(1)}, bf16[2,8,128,128]{3,2,1,0:T(8,128)(2,1)S(1)}, u32[]{:S(2)}, u32[]{:S(2)}) collective-permute-start(bf16[2,8,128,128]{3,2,1,0:T(8,128)(2,1)S(1)} %collective-permute-done.2), channel_id=1, source_target_pairs={{0,8},{4,36},{8,16},{12,44},{16,24},{20,52},{24,0},{28,60},{32,40}... | collective-permute-start | bytes 1572872 | tf_op jit(solution)/shard_map/ppermute | solution.py:360
  14.5 33.8 %collective-permute-start.5 = (bf16[2,2,8,128,128]{4,3,2,1,0:T(8,128)(2,1)S(1)}, bf16[2,2,8,128,128]{4,3,2,1,0:T(8,128)(2,1)}, u32[]{:S(2)}, u32[]{:S(2)}) collective-permute-start(bf16[2,2,8,128,128]{4,3,2,1,0:T(8,128)(2,1)S(1)} %pad_maximum_fusion), channel_id=1, source_target_pairs={{0,32},{4,12},{8,40},{12,20},{16,48},{20,28},{24,56},{28,4},{32,64... | collective-permute-start | bytes 3145736 | tf_op jit(solution)/shard_map/ppermute | solution.py:360
  16.6 14.7 %collective-permute-start.17 = (bf16[2,64,512]{2,1,0:T(8,128)(2,1)S(1)}, bf16[2,64,512]{2,1,0:T(8,128)(2,1)S(1)}, u32[]{:S(2)}, u32[]{:S(2)}) collective-permute-start(bf16[2,64,512]{2,1,0:T(8,128)(2,1)S(1)} %broadcast_select_fusion.6), channel_id=1, source_target_pairs={{0,4},{4,0},{1,5},{5,1},{2,6},{6,2},{3,7},{7,3},{8,12},{12,8},{9,1... | collective-permute-start | bytes 393224 | tf_op jit(solution)/shard_map/ppermute | solution.py:391
  16.7 14.7 %copy-start.18 = (bf16[2,8,128,128]{3,2,1,0:T(8,128)(2,1)}, bf16[2,8,128,128]{3,2,1,0:T(8,128)(2,1)S(1)}, u32[]{:S(2)}) copy-start(bf16[2,8,128,128]{3,2,1,0:T(8,128)(2,1)S(1)} %collective-permute-done.3) | copy-start | bytes 1572868
  30.0 1.3 copy-start.19
  31.3 10.2 %copy-start.22 = (f32[2]{0:T(128)S(1)}, f32[2]{0:T(128)}, u32[]{:S(2)}) copy-start(f32[2]{0:T(128)} %param.14) | copy-start | bytes 28
  31.3 20.8 %copy-start.23 = (f32[128]{0:T(128)S(1)}, f32[128]{0:T(128)}, u32[]{:S(2)}) copy-start(f32[128]{0:T(128)} %param.15) | copy-start | bytes 1540
  31.3 26.5 %collective-permute-start.8 = (bf16[2,2,8,128,128]{4,3,2,1,0:T(8,128)(2,1)}, bf16[2,2,8,128,128]{4,3,2,1,0:T(8,128)(2,1)}, u32[]{:S(2)}, u32[]{:S(2)}) collective-permute-start(bf16[2,2,8,128,128]{4,3,2,1,0:T(8,128)(2,1)} %pad_maximum_fusion.1), channel_id=1, source_target_pairs={{0,96},{4,28},{8,104},{12,4},{16,112},{20,12},{24,120},{28,20},{32... | collective-permute-start | bytes 3145736 | tf_op jit(solution)/shard_map/ppermute | solution.py:360
  31.4 7.7 %collective-permute-start.18 = (bf16[2,128,512]{2,1,0:T(8,128)(2,1)S(1)}, bf16[2,128,512]{2,1,0:T(8,128)(2,1)S(1)}, u32[]{:S(2)}, u32[]{:S(2)}) collective-permute-start(bf16[2,128,512]{2,1,0:T(8,128)(2,1)S(1)} %get-tuple-element.36), channel_id=1, source_target_pairs={{0,8},{4,36},{8,16},{12,44},{16,24},{20,52},{24,0},{28,60},{32,40}... | collective-permute-start | bytes 786440 | tf_op jit(solution)/shard_map/ppermute | solution.py:360
  31.5 9.9 %collective-permute-start.19 = (bf16[2,128,512]{2,1,0:T(8,128)(2,1)S(1)}, bf16[2,128,512]{2,1,0:T(8,128)(2,1)S(1)}, u32[]{:S(2)}, u32[]{:S(2)}) collective-permute-start(bf16[2,128,512]{2,1,0:T(8,128)(2,1)S(1)} %get-tuple-element.36), channel_id=1, source_target_pairs={{0,24},{4,100},{8,0},{12,108},{16,8},{20,116},{24,16},{28,124},{32... | collective-permute-start | bytes 786440 | tf_op jit(solution)/shard_map/ppermute | solution.py:360
  34.7 40.1 %collective-permute-start.6 = (bf16[2,2,8,128,128]{4,3,2,1,0:T(8,128)(2,1)S(1)}, bf16[2,2,8,128,128]{4,3,2,1,0:T(8,128)(2,1)}, u32[]{:S(2)}, u32[]{:S(2)}) collective-permute-start(bf16[2,2,8,128,128]{4,3,2,1,0:T(8,128)(2,1)S(1)} %pad_maximum_fusion), channel_id=1, source_target_pairs={{0,96},{4,28},{8,104},{12,4},{16,112},{20,12},{24,120},{28,20},{32... | collective-permute-start | bytes 3145736 | tf_op jit(solution)/shard_map/ppermute | solution.py:360
  39.1 7.2 %collective-permute-start.1 = (bf16[4,128,128]{2,1,0:T(8,128)(2,1)S(1)}, bf16[4,128,128]{2,1,0:T(8,128)(2,1)S(1)}, u32[]{:S(2)}, u32[]{:S(2)}) collective-permute-start(bf16[4,128,128]{2,1,0:T(8,128)(2,1)S(1)} %slice.81), channel_id=1, source_target_pairs={{0,120},{8,112},{16,104},{24,96},{32,88},{40,80},{48,72},{56,64},{... | collective-permute-start | bytes 393224 | tf_op jit(solution)/shard_map/ppermute | solution.py:411
  41.4 14.8 %collective-permute-start.20 = (bf16[2,128,512]{2,1,0:T(8,128)(2,1)S(1)}, bf16[2,128,512]{2,1,0:T(8,128)(2,1)S(1)}, u32[]{:S(2)}, u32[]{:S(2)}) collective-permute-start(bf16[2,128,512]{2,1,0:T(8,128)(2,1)S(1)} %collective-permute-done.18), channel_id=1, source_target_pairs={{0,8},{4,36},{8,16},{12,44},{16,24},{20,52},{24,0},{28,60},{32,40}... | collective-permute-start | bytes 786440 | tf_op jit(solution)/shard_map/ppermute | solution.py:360
  46.3 44.4 %collective-permute-start.7 = (bf16[2,2,8,128,128]{4,3,2,1,0:T(8,128)(2,1)}, bf16[2,2,8,128,128]{4,3,2,1,0:T(8,128)(2,1)}, u32[]{:S(2)}, u32[]{:S(2)}) collective-permute-start(bf16[2,2,8,128,128]{4,3,2,1,0:T(8,128)(2,1)} %pad_maximum_fusion.1), channel_id=1, source_target_pairs={{0,32},{4,12},{8,40},{12,20},{16,48},{20,28},{24,56},{28,4},{32,64... | collective-permute-start | bytes 3145736 | tf_op jit(solution)/shard_map/ppermute | solution.py:360
  48.3 42.7 %collective-permute-start.9 = (bf16[2,2,8,128,128]{4,3,2,1,0:T(8,128)(2,1)}, bf16[2,2,8,128,128]{4,3,2,1,0:T(8,128)(2,1)}, u32[]{:S(2)}, u32[]{:S(2)}) collective-permute-start(bf16[2,2,8,128,128]{4,3,2,1,0:T(8,128)(2,1)} %collective-permute-done.5.refs_5_), channel_id=1, source_target_pairs={{0,32},{4,12},{8,40},{12,20},{16,48},{20,28},{24,56},{28,4},{32,64... | collective-permute-start | bytes 3145736 | tf_op jit(solution)/shard_map/ppermute | solution.py:360
  52.0 7.3 %copy-start.24 = (pred[128]{0:T(512)(128)(4,1)S(1)}, pred[128]{0:T(512)(128)(4,1)}, u32[]{:S(2)}) copy-start(pred[128]{0:T(512)(128)(4,1)} %constant.354.clone.1) | copy-start | bytes 388
  56.2 11.2 %collective-permute-start.30 = (bf16[128,2048]{1,0:T(8,128)(2,1)}, bf16[128,2048]{1,0:T(8,128)(2,1)}, u32[]{:S(2)}, u32[]{:S(2)}) collective-permute-start(bf16[128,2048]{1,0:T(8,128)(2,1)} %refs_0_.1), channel_id=1, source_target_pairs={{0,1},{1,2},{2,3},{3,0},{4,5},{5,6},{6,7},{7,4},{8,9},{9,10},{10,1... | collective-permute-start | bytes 1572872 | tf_op jit(solution)/shard_map/ppermute | solution.py:388
  57.8 46.7 %collective-permute-start.10 = (bf16[2,2,8,128,128]{4,3,2,1,0:T(8,128)(2,1)}, bf16[2,2,8,128,128]{4,3,2,1,0:T(8,128)(2,1)}, u32[]{:S(2)}, u32[]{:S(2)}) collective-permute-start(bf16[2,2,8,128,128]{4,3,2,1,0:T(8,128)(2,1)} %collective-permute-done.8.refs_3_), channel_id=1, source_target_pairs={{0,96},{4,28},{8,104},{12,4},{16,112},{20,12},{24,120},{28,20},{32... | collective-permute-start | bytes 3145736 | tf_op jit(solution)/shard_map/ppermute | solution.py:360
  66.9 24.1 %copy-start = (bf16[4,2,128,512]{3,2,1,0:T(8,128)(2,1)}, bf16[4,2,128,512]{3,2,1,0:T(8,128)(2,1)S(1)}, u32[]{:S(2)}) copy-start(bf16[4,2,128,512]{3,2,1,0:T(8,128)(2,1)S(1)} %pad_maximum_fusion.2.refs_7_.refs_8_) | copy-start | bytes 3145732
  67.4 46.0 %collective-permute-start.21 = (bf16[4,2,128,512]{3,2,1,0:T(8,128)(2,1)S(1)}, bf16[4,2,128,512]{3,2,1,0:T(8,128)(2,1)S(1)}, u32[]{:S(2)}, u32[]{:S(2)}) collective-permute-start(bf16[4,2,128,512]{3,2,1,0:T(8,128)(2,1)S(1)} %pad_maximum_fusion.2.refs_7_.refs_8_), channel_id=1, source_target_pairs={{0,32},{4,12},{8,40},{12,20},{16,48},{20,28},{24,56},{28,4},{32,64... | collective-permute-start | bytes 3145736 | tf_op jit(solution)/shard_map/ppermute | solution.py:360
  74.8 44.4 %collective-permute-start.22 = (bf16[4,2,128,512]{3,2,1,0:T(8,128)(2,1)S(1)}, bf16[4,2,128,512]{3,2,1,0:T(8,128)(2,1)S(1)}, u32[]{:S(2)}, u32[]{:S(2)}) collective-permute-start(bf16[4,2,128,512]{3,2,1,0:T(8,128)(2,1)S(1)} %pad_maximum_fusion.2.refs_7_.refs_8_), channel_id=1, source_target_pairs={{0,96},{4,28},{8,104},{12,4},{16,112},{20,12},{24,120},{28,20},{32... | collective-permute-start | bytes 3145736 | tf_op jit(solution)/shard_map/ppermute | solution.py:360
  90.6 22.1 %collective-permute-start.32 = (bf16[128,2048]{1,0:T(8,128)(2,1)}, bf16[128,2048]{1,0:T(8,128)(2,1)}, u32[]{:S(2)}, u32[]{:S(2)}) collective-permute-start(bf16[128,2048]{1,0:T(8,128)(2,1)} %collective-permute-done.30.refs_0_), channel_id=1, source_target_pairs={{0,1},{1,2},{2,3},{3,0},{4,5},{5,6},{6,7},{7,4},{8,9},{9,10},{10,1... | collective-permute-start | bytes 1572872 | tf_op jit(solution)/shard_map/ppermute | solution.py:388
  91.0 30.7 %collective-permute-start.25 = (bf16[4,2,128,512]{3,2,1,0:T(8,128)(2,1)S(1)}, bf16[4,2,128,512]{3,2,1,0:T(8,128)(2,1)}, u32[]{:S(2)}, u32[]{:S(2)}) collective-permute-start(bf16[4,2,128,512]{3,2,1,0:T(8,128)(2,1)S(1)} %pad_maximum_fusion.2.refs_7_.refs_8_), channel_id=1, source_target_pairs={{0,4},{4,0},{1,5},{5,1},{2,6},{6,2},{3,7},{7,3},{8,12},{12,8},{9,1... | collective-permute-start | bytes 3145736 | tf_op jit(solution)/shard_map/ppermute | solution.py:391
  108.5 13.1 %copy-start.16 = (bf16[512,128]{1,0:T(8,128)(2,1)S(1)}, bf16[512,128]{1,0:T(8,128)(2,1)}, u32[]{:S(2)}) copy-start(bf16[512,128]{1,0:T(8,128)(2,1)} %get-tuple-element.23) | copy-start | bytes 393220
  109.4 9.9 %collective-permute-start.11 = (bf16[512,128]{1,0:T(8,128)(2,1)S(1)}, bf16[512,128]{1,0:T(8,128)(2,1)S(1)}, u32[]{:S(2)}, u32[]{:S(2)}) collective-permute-start(bf16[512,128]{1,0:T(8,128)(2,1)S(1)} %broadcast_select_fusion.10), channel_id=1, source_target_pairs={{4,0},{12,8},{20,16},{28,24},{36,32},{44,40},{52,48},{60,56},{68,6... | collective-permute-start | bytes 393224 | tf_op jit(solution)/shard_map/ppermute | solution.py:485
  112.8 7.7 %collective-permute-start.12 = (bf16[512,128]{1,0:T(8,128)(2,1)}, bf16[512,128]{1,0:T(8,128)(2,1)S(1)}, u32[]{:S(2)}, u32[]{:S(2)}) collective-permute-start(bf16[512,128]{1,0:T(8,128)(2,1)} %get-tuple-element.24), channel_id=1, source_target_pairs={{4,124},{12,116},{20,108},{28,100},{36,92},{44,84},{52,76},{60,68}... | collective-permute-start | bytes 393224 | tf_op jit(solution)/shard_map/ppermute | solution.py:484
  113.5 8.2 %copy-start.1 = (bf16[4,2,128,512]{3,2,1,0:T(8,128)(2,1)}, bf16[4,2,128,512]{3,2,1,0:T(8,128)(2,1)S(1)}, u32[]{:S(2)}) copy-start(bf16[4,2,128,512]{3,2,1,0:T(8,128)(2,1)S(1)} %collective-permute-done.21.refs_8_.refs_9_) | copy-start | bytes 3145732
  113.5 28.2 %collective-permute-start.26 = (bf16[4,2,128,512]{3,2,1,0:T(8,128)(2,1)S(1)}, bf16[4,2,128,512]{3,2,1,0:T(8,128)(2,1)S(1)}, u32[]{:S(2)}, u32[]{:S(2)}) collective-permute-start(bf16[4,2,128,512]{3,2,1,0:T(8,128)(2,1)S(1)} %collective-permute-done.21.refs_8_.refs_9_), channel_id=1, source_target_pairs={{0,4},{4,0},{1,5},{5,1},{2,6},{6,2},{3,7},{7,3},{8,12},{12,8},{9,1... | collective-permute-start | bytes 3145736 | tf_op jit(solution)/shard_map/ppermute | solution.py:391
  119.2 2.4 %copy-start.2 = (bf16[4,2,128,512]{3,2,1,0:T(8,128)(2,1)}, bf16[4,2,128,512]{3,2,1,0:T(8,128)(2,1)S(1)}, u32[]{:S(2)}) copy-start(bf16[4,2,128,512]{3,2,1,0:T(8,128)(2,1)S(1)} %collective-permute-done.22.refs_9_.refs_10_) | copy-start | bytes 3145732
  119.2 22.6 %collective-permute-start.27 = (bf16[4,2,128,512]{3,2,1,0:T(8,128)(2,1)S(1)}, bf16[4,2,128,512]{3,2,1,0:T(8,128)(2,1)S(1)}, u32[]{:S(2)}, u32[]{:S(2)}) collective-permute-start(bf16[4,2,128,512]{3,2,1,0:T(8,128)(2,1)S(1)} %collective-permute-done.22.refs_9_.refs_10_), channel_id=1, source_target_pairs={{0,4},{4,0},{1,5},{5,1},{2,6},{6,2},{3,7},{7,3},{8,12},{12,8},{9,1... | collective-permute-start | bytes 3145736 | tf_op jit(solution)/shard_map/ppermute | solution.py:391
  119.4 9.4 %collective-permute-start.23 = (bf16[2,2,128,512]{3,2,1,0:T(8,128)(2,1)S(1)}, bf16[2,2,128,512]{3,2,1,0:T(8,128)(2,1)}, u32[]{:S(2)}, u32[]{:S(2)}) collective-permute-start(bf16[2,2,128,512]{3,2,1,0:T(8,128)(2,1)S(1)} %slice.89), channel_id=1, source_target_pairs={{0,32},{4,12},{8,40},{12,20},{16,48},{20,28},{24,56},{28,4},{32,64... | collective-permute-start | bytes 1572872 | tf_op jit(solution)/shard_map/ppermute | solution.py:360
  120.5 10.9 %collective-permute-start.24 = (bf16[2,2,128,512]{3,2,1,0:T(8,128)(2,1)S(1)}, bf16[2,2,128,512]{3,2,1,0:T(8,128)(2,1)}, u32[]{:S(2)}, u32[]{:S(2)}) collective-permute-start(bf16[2,2,128,512]{3,2,1,0:T(8,128)(2,1)S(1)} %slice.90), channel_id=1, source_target_pairs={{0,96},{4,28},{8,104},{12,4},{16,112},{20,12},{24,120},{28,20},{32... | collective-permute-start | bytes 1572872 | tf_op jit(solution)/shard_map/ppermute | solution.py:360
  121.7 34.3 %copy-start.7 = (bf16[512,256]{1,0:T(8,128)(2,1)}, bf16[512,256]{1,0:T(8,128)(2,1)S(1)}, u32[]{:S(2)}) copy-start(bf16[512,256]{1,0:T(8,128)(2,1)S(1)} %pad_maximum_fusion.7.refs_1_.refs_2_) | copy-start | bytes 786436
  121.7 11.2 %collective-permute-start.13 = (bf16[512,256]{1,0:T(8,128)(2,1)S(1)}, bf16[512,256]{1,0:T(8,128)(2,1)S(1)}, u32[]{:S(2)}, u32[]{:S(2)}) collective-permute-start(bf16[512,256]{1,0:T(8,128)(2,1)S(1)} %pad_maximum_fusion.7.refs_1_.refs_2_), channel_id=1, source_target_pairs={{0,1},{1,2},{2,3},{3,0},{4,5},{5,6},{6,7},{7,4},{8,9},{9,10},{10,1... | collective-permute-start | bytes 786440 | tf_op jit(solution)/shard_map/ppermute | solution.py:388
  128.7 8.6 %collective-permute-start.14 = (bf16[512,256]{1,0:T(8,128)(2,1)S(1)}, bf16[512,256]{1,0:T(8,128)(2,1)S(1)}, u32[]{:S(2)}, u32[]{:S(2)}) collective-permute-start(bf16[512,256]{1,0:T(8,128)(2,1)S(1)} %pad_maximum_fusion.7.refs_1_.refs_2_), channel_id=1, source_target_pairs={{0,3},{1,0},{2,1},{3,2},{4,7},{5,4},{6,5},{7,6},{8,11},{9,8},{10,9... | collective-permute-start | bytes 786440 | tf_op jit(solution)/shard_map/ppermute | solution.py:388
  131.4 15.3 %collective-permute-start.28 = (bf16[2,2,128,512]{3,2,1,0:T(8,128)(2,1)}, bf16[2,2,128,512]{3,2,1,0:T(8,128)(2,1)S(1)}, u32[]{:S(2)}, u32[]{:S(2)}) collective-permute-start(bf16[2,2,128,512]{3,2,1,0:T(8,128)(2,1)} %collective-permute-done.23.refs_10_.refs_11_), channel_id=1, source_target_pairs={{0,4},{4,0},{1,5},{5,1},{2,6},{6,2},{3,7},{7,3},{8,12},{12,8},{9,1... | collective-permute-start | bytes 1572872 | tf_op jit(solution)/shard_map/ppermute | solution.py:391
  132.9 8.9 %copy-start.8 = (bf16[512,256]{1,0:T(8,128)(2,1)}, bf16[512,256]{1,0:T(8,128)(2,1)S(1)}, u32[]{:S(2)}) copy-start(bf16[512,256]{1,0:T(8,128)(2,1)S(1)} %collective-permute-done.13.refs_2_.refs_3_) | copy-start | bytes 786436
  132.9 13.8 %collective-permute-start.29 = (bf16[2,2,128,512]{3,2,1,0:T(8,128)(2,1)}, bf16[2,2,128,512]{3,2,1,0:T(8,128)(2,1)S(1)}, u32[]{:S(2)}, u32[]{:S(2)}) collective-permute-start(bf16[2,2,128,512]{3,2,1,0:T(8,128)(2,1)} %collective-permute-done.24.refs_11_.refs_12_), channel_id=1, source_target_pairs={{0,4},{4,0},{1,5},{5,1},{2,6},{6,2},{3,7},{7,3},{8,12},{12,8},{9,1... | collective-permute-start | bytes 1572872 | tf_op jit(solution)/shard_map/ppermute | solution.py:391
  137.3 4.5 %copy-start.9 = (bf16[512,256]{1,0:T(8,128)(2,1)}, bf16[512,256]{1,0:T(8,128)(2,1)S(1)}, u32[]{:S(2)}) copy-start(bf16[512,256]{1,0:T(8,128)(2,1)S(1)} %collective-permute-done.14.refs_3_.refs_4_) | copy-start | bytes 786436
  137.3 30.9 %collective-permute-start.31 = (bf16[128,2048]{1,0:T(8,128)(2,1)}, bf16[128,2048]{1,0:T(8,128)(2,1)}, u32[]{:S(2)}, u32[]{:S(2)}) collective-permute-start(bf16[128,2048]{1,0:T(8,128)(2,1)} %refs_0_.1), channel_id=1, source_target_pairs={{0,3},{1,0},{2,1},{3,2},{4,7},{5,4},{6,5},{7,6},{8,11},{9,8},{10,9... | collective-permute-start | bytes 1572872 | tf_op jit(solution)/shard_map/ppermute | solution.py:388
  141.7 1.0 copy-start.3
  141.7 7.2 %collective-permute-start.15 = (bf16[256,256]{1,0:T(8,128)(2,1)}, bf16[256,256]{1,0:T(8,128)(2,1)S(1)}, u32[]{:S(2)}, u32[]{:S(2)}) collective-permute-start(bf16[256,256]{1,0:T(8,128)(2,1)} %slice.85), channel_id=1, source_target_pairs={{0,1},{1,2},{2,3},{3,0},{4,5},{5,6},{6,7},{7,4},{8,9},{9,10},{10,1... | collective-permute-start | bytes 393224 | tf_op jit(solution)/shard_map/ppermute | solution.py:388
  142.6 1.0 copy-start.4
  143.6 12.4 %collective-permute-start.16 = (bf16[256,256]{1,0:T(8,128)(2,1)S(1)}, bf16[256,256]{1,0:T(8,128)(2,1)S(1)}, u32[]{:S(2)}, u32[]{:S(2)}) collective-permute-start(bf16[256,256]{1,0:T(8,128)(2,1)S(1)} %slice.86), channel_id=1, source_target_pairs={{0,3},{1,0},{2,1},{3,2},{4,7},{5,4},{6,5},{7,6},{8,11},{9,8},{10,9... | collective-permute-start | bytes 393224 | tf_op jit(solution)/shard_map/ppermute | solution.py:388
  146.7 9.3 %copy-start.5 = (bf16[2,2,128,512]{3,2,1,0:T(8,128)(2,1)}, bf16[2,2,128,512]{3,2,1,0:T(8,128)(2,1)S(1)}, u32[]{:S(2)}) copy-start(bf16[2,2,128,512]{3,2,1,0:T(8,128)(2,1)S(1)} %collective-permute-done.28.refs_15_.refs_16_) | copy-start | bytes 1572868
  146.7 9.3 %copy-start.6 = (bf16[2,2,128,512]{3,2,1,0:T(8,128)(2,1)}, bf16[2,2,128,512]{3,2,1,0:T(8,128)(2,1)S(1)}, u32[]{:S(2)}) copy-start(bf16[2,2,128,512]{3,2,1,0:T(8,128)(2,1)S(1)} %collective-permute-done.29.refs_16_.refs_17_) | copy-start | bytes 1572868
  148.9 7.1 %copy-start.11 = (bf16[256,256]{1,0:T(8,128)(2,1)}, bf16[256,256]{1,0:T(8,128)(2,1)S(1)}, u32[]{:S(2)}) copy-start(bf16[256,256]{1,0:T(8,128)(2,1)S(1)} %collective-permute-done.15.refs_4_.refs_5_) | copy-start | bytes 393220
  156.0 0.6 copy-start.12
  164.4 12.3 %collective-permute-start.35 = (bf16[64,2048]{1,0:T(8,128)(2,1)}, bf16[64,2048]{1,0:T(8,128)(2,1)S(1)}, u32[]{:S(2)}, u32[]{:S(2)}) collective-permute-start(bf16[64,2048]{1,0:T(8,128)(2,1)} %get-tuple-element.28), channel_id=1, source_target_pairs={{0,3},{1,0},{2,1},{3,2},{4,7},{5,4},{6,5},{7,6},{8,11},{9,8},{10,9... | collective-permute-start | bytes 786440 | tf_op jit(solution)/shard_map/ppermute | solution.py:388
  168.2 13.0 %collective-permute-start.33 = (bf16[64,2048]{1,0:T(8,128)(2,1)}, bf16[64,2048]{1,0:T(8,128)(2,1)S(1)}, u32[]{:S(2)}, u32[]{:S(2)}) collective-permute-start(bf16[64,2048]{1,0:T(8,128)(2,1)} %get-tuple-element.26), channel_id=1, source_target_pairs={{0,1},{1,2},{2,3},{3,0},{4,5},{5,6},{6,7},{7,4},{8,9},{9,10},{10,1... | collective-permute-start | bytes 786440 | tf_op jit(solution)/shard_map/ppermute | solution.py:388
  176.7 4.5 %copy-start.13 = (bf16[128,2048]{1,0:T(8,128)(2,1)S(1)}, bf16[128,2048]{1,0:T(8,128)(2,1)}, u32[]{:S(2)}) copy-start(bf16[128,2048]{1,0:T(8,128)(2,1)} %get-tuple-element.25) | copy-start | bytes 1572868
  177.9 13.9 %collective-permute-start.36 = (bf16[128,2048]{1,0:T(8,128)(2,1)S(1)}, bf16[128,2048]{1,0:T(8,128)(2,1)S(1)}, u32[]{:S(2)}, u32[]{:S(2)}) collective-permute-start(bf16[128,2048]{1,0:T(8,128)(2,1)S(1)} %add_convert_fusion.1), channel_id=1, source_target_pairs={{0,3},{1,0},{2,1},{3,2},{4,7},{5,4},{6,5},{7,6},{8,11},{9,8},{10,9... | collective-permute-start | bytes 1572872 | tf_op jit(solution)/shard_map/ppermute | solution.py:388
  181.3 14.3 %collective-permute-start.34 = (bf16[128,2048]{1,0:T(8,128)(2,1)S(1)}, bf16[128,2048]{1,0:T(8,128)(2,1)S(1)}, u32[]{:S(2)}, u32[]{:S(2)}) collective-permute-start(bf16[128,2048]{1,0:T(8,128)(2,1)S(1)} %add_convert_fusion.2), channel_id=1, source_target_pairs={{0,1},{1,2},{2,3},{3,0},{4,5},{5,6},{6,7},{7,4},{8,9},{9,10},{10,1... | collective-permute-start | bytes 1572872 | tf_op jit(solution)/shard_map/ppermute | solution.py:388
where the time goes:
time: 198 us
  starting transfers between devices  64.2 us (32%)
  Pallas kernels  61.9 us (31%)
  waiting for transfers between devices  53 us (27%)
  other arithmetic  8.96 us (5%)
  local copies, waits for them, and re-layouts  7.88 us (4%)
    pallas_call x4, Pallas kernels, attend(): pl.pallas_call(functools.partial(attend_kernel, spans, edge, last), out_s...  37.5 us
    ppermute x16, starting transfers between devices, passed(): return lax.ppermute(array, SEQ, PAIRS[axis, step])  29.4 us
    ppermute x16, waiting for transfers between devices, passed(): return lax.ppermute(array, SEQ, PAIRS[axis, step])  27.2 us
    pallas_call x3, Pallas kernels, token_parts(): pl.pallas_call(functools.partial(token_kernel, steps), out_shape=[jax.Sha...  24.4 us
    ppermute x11, starting transfers between devices, along_x(): return lax.ppermute(array, 'x', [(i, (i + step) % 4) for i in range(4)])  19.9 us
    ppermute x11, waiting for transfers between devices, along_x(): return lax.ppermute(array, 'x', [(i, (i + step) % 4) for i in range(4)])  19.9 us
    ppermute x7, starting transfers between devices, swapped(): return lax.ppermute(array, 'c', swap)  9.77 us
    ppermute x1, waiting for transfers between devices, per_device(): high = lax.ppermute(odd[8:], ('z', 'y'), [(i, 15 - i) for i in range(16)])  4.21 us
  transfers between devices with their start and end apart: 37, of which 13 were waited for; matrix products, arithmetic and copies ran while one was open for 5% of the time, Pallas kernels for 31%

commit v1 on v0

--- a/solution.py
+++ b/solution.py
@@ -21,7 +21,7 @@
 ROWS = DV + 16
 
 
-def attend_kernel(spans, edge, last, ids_ref, lam_ref, q_ref, gain_ref, *refs):
+def attend_kernel(spans, at, edge, last, ids_ref, lam_ref, q_ref, gain_ref, *refs):
     first = edge == "own"
     if not first:
         top_in, acc_in, *refs = refs
@@ -30,7 +30,7 @@
         low_ref, high_ref, tops, acc, *refs = refs
     else:
         tops, acc, *refs = refs
-    held, sems, items, scores_a, scores_b, peaks_a, peaks_b = refs
+    held, sems, items, seen, scores_a, scores_b, peaks_a, peaks_b = refs
     own = ids_ref[0]
     slots = held.shape[0]
     slot = 0
@@ -45,8 +45,7 @@
         tops[...] = top_in[...]
         acc[...] = acc_in[...]
 
-    for slot in range(slots):
-        pltpu.make_async_copy(held.at[slot], held.at[slot], sems.at[slot]).wait()
+    seen[0] = 0
 
     units = [(t, m) for t in range(HALF // TILE) for m in range(2)]
     parts = 2 * HALF // TILE
@@ -100,29 +99,42 @@
         while steps:
             steps = [s for s in steps if next(s, True) is None]
 
-    def listed(i, count):
-        for side, limit in ((0, own), (1, 15 - own)):
-            items[count] = 2 * i + side
-            count = count + (ids_ref[1 + i] < limit).astype(jnp.int32)
+    def listed():
+        count = jnp.int32(0)
+        for i in range(slots):
+            for side, limit in ((0, own), (1, 15 - own)):
+                items[count] = 2 * i + side
+                count = count + (ids_ref[at[i]] < limit).astype(jnp.int32)
         return count
+
+    def ready(item):
+        def one(slot, carry):
+            pltpu.make_async_copy(held.at[slot], held.at[slot], sems.at[slot]).wait()
+            return carry
+
+        lax.fori_loop(seen[0], item // 2 + 1, one, 0)
+        seen[0] = jnp.maximum(seen[0], item // 2 + 1)
 
     def pair(k, carry):
         one, two, three = items[2 * k], items[2 * k + 1], items[2 * k + 2]
+        ready(two)
         together(score_steps(two, scores_b, peaks_b), weight_steps(one, scores_a, peaks_a))
 
         @pl.when(2 * k + 1 < count)
         def _():
+            ready(three)
             together(score_steps(three, scores_a, peaks_a), weight_steps(two, scores_b, peaks_b))
 
         return carry
 
     if not first:
-        count = lax.fori_loop(0, slots, listed, jnp.int32(0))
+        count = listed()
         items[count] = 0
         items[count + 1] = 0
 
         @pl.when(count > 0)
         def _():
+            ready(items[0])
             together(score_steps(items[0], scores_a, peaks_a))
 
         lax.fori_loop(0, (count + 1) // 2, pair, 0)
@@ -153,23 +165,25 @@
 
         lax.fori_loop(0, HALF // TILE, tile, 0)
 
+    ready(2 * slots - 2)
     if edge == "own":
-        edge_item(0, 0, 0)
-
-        @pl.when(own < 15 - own)
+
+
+        def own_side(side, carry):
+            edge_item(0, side, side * 2 * HALF)
+            return carry
+
+        lax.fori_loop(0, 1 + (own < 15 - own).astype(jnp.int32), own_side, 0)
+
+    if edge == "other":
+
+        here = jnp.int32(-1)
+        for i in range(slots):
+            here = jnp.where(ids_ref[at[i]] == 15 - own, i, here)
+
+        @pl.when(here >= 0)
         def _():
-            edge_item(0, 1, 2 * HALF)
-
-    if edge == "other":
-
-        def edges(i, carry):
-            @pl.when(ids_ref[1 + i] == 15 - own)
-            def _():
-                edge_item(i, 1, HALF)
-
-            return carry
-
-        lax.fori_loop(0, slots, edges, 0)
+            edge_item(here, 1, HALF)
 
     if last:
         for t in range(2 * HALF // TILE):
@@ -180,10 +194,10 @@
             spread = lax.rsqrt(jnp.mean(differ * differ, axis=0, keepdims=True) + 1e-06)
             out_ref = low_ref if t * TILE < HALF else high_ref
             rows = slice(t * TILE % HALF, t * TILE % HALF + TILE)
-            out_ref[rows, :] = (differ * spread * gain_ref[...]).T.astype(BF16)
-
-
-def attend(slots, ids, lam, query, gain, state, edge, last):
+            out_ref[rows, :] = ((differ * spread).T * gain_ref[...]).astype(BF16)
+
+
+def attend(slots, at, ids, lam, query, gain, state, edge, last):
     pieces = [p if p.ndim == 5 else p[None] for p in slots]
     spans = tuple(p.shape[0] for p in pieces)
     count = sum(spans)
@@ -193,6 +207,7 @@
         pltpu.VMEM((count, 2, 8, DV, DV), BF16),
         pltpu.SemaphoreType.DMA((count,)),
         pltpu.SMEM((2 * count + 2,), jnp.int32),
+        pltpu.SMEM((1,), jnp.int32),
         pltpu.VMEM((4, 2 * HALF, TILE), F32),
         pltpu.VMEM((4, 2 * HALF, TILE), F32),
         pltpu.VMEM((4, 8, TILE), F32),
@@ -210,7 +225,7 @@
     state = [] if state is None else list(state)
     flops = count * 2 * HALF * HALF * 2 * 2 * 2 * (DV + DV) // 2
     return pl.pallas_call(
-        functools.partial(attend_kernel, spans, edge, last),
+        functools.partial(attend_kernel, spans, at, edge, last),
         out_shape=out_shape,
         in_specs=[smem, smem, vmem, vmem]
         + [vmem] * len(state)
@@ -220,6 +235,7 @@
         cost_estimate=pl.CostEstimate(
             flops=flops, bytes_accessed=count * 2**19, transcendentals=count * 2**20
         ),
+        compiler_params=pltpu.CompilerParams(vmem_limit_bytes=26 * 2**20),
         name="attend",
     )(ids, lam, query, gain, *state, *pieces)
 
@@ -273,7 +289,7 @@
             for piece in weight_refs[5 * half : 5 * half + 5]:
                 for j in range(piece.shape[0]):
                     copied(
-                        piece.at[j, kind], target.at[half, chips_ref[16 * half + slot]], 3 + kind
+                        piece.at[j, kind], target.at[half, chips_ref[1 + 16 * half + slot]], 3 + kind
                     )
                     slot += 1
 
@@ -336,6 +352,9 @@
         cost_estimate=pl.CostEstimate(
             flops=count * 128 * 2048 * 3072 * 2, bytes_accessed=12 * 2**20, transcendentals=0
         ),
+        compiler_params=pltpu.CompilerParams(
+            vmem_limit_bytes=(61 if steps == (2,) else 44) * 2**20
+        ),
         name="token_parts",
     )(x, chips, gain, *tokens, *parts)
 
@@ -390,13 +409,11 @@
     def swapped(array):
         return lax.ppermute(array, "c", swap)
 
-    scaled = queries * jnp.asarray(DQK ** (-0.5), BF16)
-
     def packed(head):
         cols = slice(head * DV, (head + 1) * DV)
         k = keys[:, cols].reshape(4, DV, DV)
         v = values[:, cols].reshape(4, DV, DV)
-        q = scaled[:, cols].reshape(4, DV, DV)
+        q = queries[:, cols].reshape(4, DV, DV)
         return jnp.concatenate([k, jnp.swapaxes(v, 1, 2), q], axis=0)
 
     head_a, head_b = packed(0), packed(1)
@@ -410,6 +427,7 @@
 
     high = lax.ppermute(odd[8:], ("z", "y"), [(i, 15 - i) for i in range(16)])
     query = jnp.concatenate([even[8:].reshape(HALF, DV), high.reshape(HALF, DV)], axis=0).T
+    query = query * jnp.asarray(DQK ** (-0.5), BF16)
     none = jnp.zeros((DQK, 2 * HALF), BF16)
     query = jnp.stack(
         [
@@ -419,12 +437,19 @@
     )
 
     lam = jnp.where(first, lambdas[0:1], lambdas[1:2])
-    gain = head_gain[:, None]
+    gain = head_gain[None]
+
+    near = (0, -1, 1, 2)
+    order = [(a, b) for b in (0, -1, 1, 2) for a in near]
+    offsets = [jnp.asarray([p[n] for p in order], jnp.int32) for n in range(2)]
+    table = jnp.concatenate(
+        [chip[None]] + [source_chip(*offsets, core) for core in (0, 1)]
+    ).astype(jnp.int32)
 
     def attending(slots, state, edge=None, last=False):
         places = [p for place, _ in slots for p in (place if isinstance(place[0], tuple) else (place,))]
-        ids = jnp.stack([chip] + [source_chip(*place) for place in places])
-        return attend([c for _, c in slots], ids, lam, query, gain, state, edge, last)
+        at = tuple(1 + order.index(place) for place in places)
+        return attend([c for _, c in slots], at, table, lam, query, gain, state, edge, last)
 
     near_p, near_n = passed(chunk, 1, 1), passed(chunk, 1, -1)
     state = attending([((0, 0), chunk)], None, "own")
@@ -464,15 +489,6 @@
     row_a, row_b = passed(row_p[:2], 2, 1), passed(row_n[2:], 2, -1)
     weights = [row, row_p, row_n, row_a, row_b]
     weights += [swapped(w) for w in weights]
-    near = (0, -1, 1, 2)
-    chips = jnp.stack(
-        [
-            source_chip(a, b, core)
-            for core in (0, 1)
-            for places in ((near, 0), (near, -1), (near, 1), (near, 2))
-            for a, b in ((n, places[1]) for n in places[0])
-        ]
-    )
     low, high = attending(
         [(((0, 2), (-1, 2)), over_p), (((1, 2), (2, 2)), over_n)], state, last=True
     )
@@ -491,10 +507,10 @@
     x = lax.axis_index("x")[None]
     parts = (attended, prev, following, far_top, far_low, out_weight, *weights)
     gain = mixer_gain[None]
-    far_top_part, far_low_part = token_parts((2,), x, chips, gain, (tokens_far,), parts)
+    far_top_part, far_low_part = token_parts((2,), x, table, gain, (tokens_far,), parts)
     from_prev = along_x(far_top_part, 1)
     from_next = along_x(far_low_part, -1)
-    prev_part, next_part = token_parts((3, 1), x, chips, gain, (tokens_p, tokens_n), parts)
+    prev_part, next_part = token_parts((3, 1), x, table, gain, (tokens_p, tokens_n), parts)
 
     def added(a, b):
         return (a.astype(F32) + b.astype(F32)).astype(BF16)
@@ -504,7 +520,7 @@
     to_prev = added(prev_part, jnp.concatenate([none, from_next], axis=0))
     got_prev = along_x(to_next, 1)
     got_next = along_x(to_prev, -1)
-    (total,) = token_parts((0,), x, chips, gain, (tokens,), parts)
+    (total,) = token_parts((0,), x, table, gain, (tokens,), parts)
     return (total + got_prev.astype(F32) + got_next.astype(F32)).astype(BF16)
 
 

time: 198 us -> 194 us (0.980)
  the two profiles are of different devices: /device:TPU:32 before, /device:TPU:22 now
where the time goes in v1:
time: 194 us; the launch traced here: 193 us
  Pallas kernels  62.7 us (32%)
  waiting for transfers between devices  59.4 us (31%)
  starting transfers between devices  47.3 us (24%)
  local copies, waits for them, and re-layouts  17.7 us (9%)
  other arithmetic  4.31 us (2%)
  between operations  1.98 us (1%)
    pallas_call x3, Pallas kernels, token_parts(): pl.pallas_call(functools.partial(token_kernel, steps), out_shape=[jax.Sha...  34.6 us
    ppermute x16, waiting for transfers between devices, passed(): return lax.ppermute(array, SEQ, PAIRS[axis, step])  29.7 us
    pallas_call x4, Pallas kernels, attend(): pl.pallas_call(functools.partial(attend_kernel, spans, at, edge, last), o...  28.1 us
    ppermute x11, waiting for transfers between devices, along_x(): return lax.ppermute(array, 'x', [(i, (i + step) % 4) for i in range(4)])  28 us
    ppermute x16, starting transfers between devices, passed(): return lax.ppermute(array, SEQ, PAIRS[axis, step])  24.8 us
    ppermute x11, starting transfers between devices, along_x(): return lax.ppermute(array, 'x', [(i, (i + step) % 4) for i in range(4)])  13.5 us
    unnamed x112, local copies, waits for them, and re-layouts  13.1 us
    ppermute x7, starting transfers between devices, swapped(): return lax.ppermute(array, 'c', swap)  5.45 us
  transfers between devices with their start and end apart: 37, of which 11 were waited for; matrix products, arithmetic and copies ran while one was open for 3% of the time, Pallas kernels for 32%

profile of v1, /device:TPU:22, one launch (start us, length us, event | category | flops | bytes accessed | tf_op | source)
XLA Modules:
  0.0 193.5 jit_solution(3702499711369321704)
XLA Ops:
  0.0 1.0 fusion.22
  1.0 1.0 fusion.21
  2.5 1.7 collective-permute-done
  4.5 1.4 collective-permute-start.2
  5.8 0.7 collective-permute-start.3
  6.6 7.2 %collective-permute-done.2 = bf16[2,8,128,128]{3,2,1,0:T(8,128)(2,1)S(1)} collective-permute-done((bf16[2,8,128,128]{3,2,1,0:T(8,128)(2,1)S(1)}, bf16[2,8,128,128]{3,2,1,0:T(8,128)(2,1)S(1)}, u32[]{:S(2)}, u32[]{:S(2)}) %collective-permute-start.2) | collective-permute-done | bytes 524320 | tf_op jit(solution)/shard_map/ppermute | solution.py:379
  13.7 1.3 collective-permute-start.4
  15.2 1.1 pad_maximum_fusion
  16.3 1.9 collective-permute-start.5
  18.2 8.1 %collective-permute-done.4 = bf16[2,8,128,128]{3,2,1,0:T(8,128)(2,1)S(1)} collective-permute-done((bf16[2,8,128,128]{3,2,1,0:T(8,128)(2,1)S(1)}, bf16[2,8,128,128]{3,2,1,0:T(8,128)(2,1)S(1)}, u32[]{:S(2)}, u32[]{:S(2)}) %collective-permute-start.4) | collective-permute-done | bytes 524320 | tf_op jit(solution)/shard_map/ppermute | solution.py:379
  26.3 1.2 pad_maximum_fusion.1
  27.5 4.0 %collective-permute-start.8 = (bf16[2,2,8,128,128]{4,3,2,1,0:T(8,128)(2,1)}, bf16[2,2,8,128,128]{4,3,2,1,0:T(8,128)(2,1)}, u32[]{:S(2)}, u32[]{:S(2)}) collective-permute-start(bf16[2,2,8,128,128]{4,3,2,1,0:T(8,128)(2,1)} %pad_maximum_fusion.1), channel_id=1, source_target_pairs={{0,96},{4,28},{8,104},{12,4},{16,112},{20,12},{24,120},{28,20},{32... | collective-permute-start | bytes 3145736 | tf_op jit(solution)/shard_map/ppermute | solution.py:379
  31.7 1.2 collective-permute-start.18
  32.9 0.9 collective-permute-start.19
  33.8 2.2 %collective-permute-start.1 = (bf16[4,128,128]{2,1,0:T(8,128)(2,1)S(1)}, bf16[4,128,128]{2,1,0:T(8,128)(2,1)S(1)}, u32[]{:S(2)}, u32[]{:S(2)}) collective-permute-start(bf16[4,128,128]{2,1,0:T(8,128)(2,1)S(1)} %slice.79), channel_id=1, source_target_pairs={{0,120},{8,112},{16,104},{24,96},{32,88},{40,80},{48,72},{56,64},{... | collective-permute-start | bytes 393224 | tf_op jit(solution)/shard_map/ppermute | solution.py:428
  36.0 2.4 %collective-permute-done.18 = bf16[2,128,512]{2,1,0:T(8,128)(2,1)S(1)} collective-permute-done((bf16[2,128,512]{2,1,0:T(8,128)(2,1)S(1)}, bf16[2,128,512]{2,1,0:T(8,128)(2,1)S(1)}, u32[]{:S(2)}, u32[]{:S(2)}) %collective-permute-start.18) | collective-permute-done | bytes 262176 | tf_op jit(solution)/shard_map/ppermute | solution.py:379
  38.4 2.9 %collective-permute-start.6 = (bf16[2,2,8,128,128]{4,3,2,1,0:T(8,128)(2,1)}, bf16[2,2,8,128,128]{4,3,2,1,0:T(8,128)(2,1)}, u32[]{:S(2)}, u32[]{:S(2)}) collective-permute-start(bf16[2,2,8,128,128]{4,3,2,1,0:T(8,128)(2,1)} %pad_maximum_fusion), channel_id=1, source_target_pairs={{0,96},{4,28},{8,104},{12,4},{16,112},{20,12},{24,120},{28,20},{32... | collective-permute-start | bytes 3145736 | tf_op jit(solution)/shard_map/ppermute | solution.py:379
  41.3 2.4 %collective-permute-done.19 = bf16[2,128,512]{2,1,0:T(8,128)(2,1)S(1)} collective-permute-done((bf16[2,128,512]{2,1,0:T(8,128)(2,1)S(1)}, bf16[2,128,512]{2,1,0:T(8,128)(2,1)S(1)}, u32[]{:S(2)}, u32[]{:S(2)}) %collective-permute-start.19) | collective-permute-done | bytes 262176 | tf_op jit(solution)/shard_map/ppermute | solution.py:379
  43.7 3.2 %collective-permute-start.20 = (bf16[2,128,512]{2,1,0:T(8,128)(2,1)S(1)}, bf16[2,128,512]{2,1,0:T(8,128)(2,1)S(1)}, u32[]{:S(2)}, u32[]{:S(2)}) collective-permute-start(bf16[2,128,512]{2,1,0:T(8,128)(2,1)S(1)} %collective-permute-done.18), channel_id=1, source_target_pairs={{0,8},{4,36},{8,16},{12,44},{16,24},{20,52},{24,0},{28,60},{32,40}... | collective-permute-start | bytes 786440 | tf_op jit(solution)/shard_map/ppermute | solution.py:379
  47.0 0.6 fusion.23
  49.3 2.4 %collective-permute-done.20 = bf16[2,128,512]{2,1,0:T(8,128)(2,1)S(1)} collective-permute-done((bf16[2,128,512]{2,1,0:T(8,128)(2,1)S(1)}, bf16[2,128,512]{2,1,0:T(8,128)(2,1)S(1)}, u32[]{:S(2)}, u32[]{:S(2)}) %collective-permute-start.20) | collective-permute-done | bytes 262176 | tf_op jit(solution)/shard_map/ppermute | solution.py:379
  51.7 0.8 collective-permute-start.30
  52.5 0.5 collective-permute-start.10
  53.3 4.4 %attend.4 = (f32[2,8,1024]{2,1,0:T(8,128)S(1)}, f32[2,144,1024]{2,1,0:T(8,128)S(1)}) custom-call(s32[33]{0:T(128)S(1)} %pad_add_fusion.ids_ref.chips_ref, f32[1]{0:T(128)S(6)} %select_n.117.lam_ref, bf16[2,128,1024]{2,1,0:T(8,128)(2,1)S(1)} %pad_maximum_fusion.3.q_ref, f32[1,128]{1,0:T(1,128)S(1)} %bitcast.50, ...), custom_call_target="tpu_custom_call" | custom-call | flops 536870912 | bytes 524288 | tf_op jit(solution)/shard_map/attend/pallas_call | solution.py:227
  57.9 7.7 %collective-permute-done.30.refs_0_ = bf16[128,2048]{1,0:T(8,128)(2,1)S(1)} collective-permute-done((bf16[128,2048]{1,0:T(8,128)(2,1)}, bf16[128,2048]{1,0:T(8,128)(2,1)S(1)}, u32[]{:S(2)}, u32[]{:S(2)}) %collective-permute-start.30) | collective-permute-done | bytes 524320 | tf_op jit(solution)/shard_map/ppermute | solution.py:407
  65.6 3.2 %collective-permute-start.22 = (bf16[4,2,128,512]{3,2,1,0:T(8,128)(2,1)S(1)}, bf16[4,2,128,512]{3,2,1,0:T(8,128)(2,1)S(1)}, u32[]{:S(2)}, u32[]{:S(2)}) collective-permute-start(bf16[4,2,128,512]{3,2,1,0:T(8,128)(2,1)S(1)} %pad_maximum_fusion.2.refs_7_.refs_8_), channel_id=1, source_target_pairs={{0,96},{4,28},{8,104},{12,4},{16,112},{20,12},{24,120},{28,20},{32... | collective-permute-start | bytes 3145736 | tf_op jit(solution)/shard_map/ppermute | solution.py:379
  68.9 11.0 %attend.5 = (f32[2,8,1024]{2,1,0:T(8,128)S(1)}, f32[2,144,1024]{2,1,0:T(8,128)S(1)}) custom-call(s32[33]{0:T(128)S(1)} %pad_add_fusion.ids_ref.chips_ref, f32[1]{0:T(128)S(6)} %select_n.117.lam_ref, bf16[2,128,1024]{2,1,0:T(8,128)(2,1)S(1)} %pad_maximum_fusion.3.q_ref, f32[1,128]{1,0:T(1,128)S(1)} %bitcast.51, f32[2,8,1024]{2,1,0:T(8,128)S(1)} %get-tuple-element.17.refs_0_, ...), custom_call_target="tpu_custom_call" | custom-call | flops 3758096384 | bytes 3670016 | tf_op jit(solution)/shard_map/attend/pallas_call | solution.py:227
  79.9 1.6 collective-permute-start.32
  81.5 5.8 %attend.6 = (f32[2,8,1024]{2,1,0:T(8,128)S(1)}, f32[2,144,1024]{2,1,0:T(8,128)S(1)}) custom-call(s32[33]{0:T(128)S(1)} %pad_add_fusion.ids_ref.chips_ref, f32[1]{0:T(128)S(6)} %select_n.117.lam_ref, bf16[2,128,1024]{2,1,0:T(8,128)(2,1)S(1)} %pad_maximum_fusion.3.q_ref, f32[1,128]{1,0:T(1,128)S(1)} %bitcast.52, f32[2,8,1024]{2,1,0:T(8,128)S(1)} %get-tuple-element.19.refs_0_, ...), custom_call_target="tpu_custom_call" | custom-call | flops 2147483648 | bytes 2097152 | tf_op jit(solution)/shard_map/attend/pallas_call | solution.py:227
  87.3 6.9 %attend.7 = (bf16[512,128]{1,0:T(8,128)(2,1)S(1)}, bf16[512,128]{1,0:T(8,128)(2,1)S(1)}) custom-call(s32[33]{0:T(128)S(1)} %pad_add_fusion.ids_ref.chips_ref, f32[1]{0:T(128)S(6)} %select_n.117.lam_ref, bf16[2,128,1024]{2,1,0:T(8,128)(2,1)S(1)} %pad_maximum_fusion.3.q_ref, f32[1,128]{1,0:T(1,128)S(1)} %bitcast.53, ...), custom_call_target="tpu_custom_call" | custom-call | flops 2147483648 | bytes 2097152 | tf_op jit(solution)/shard_map/attend/pallas_call | solution.py:227
  94.2 0.7 collective-permute-start.11
  94.9 0.7 collective-permute-start.12
  95.6 3.2 %collective-permute-start.26 = (bf16[4,2,128,512]{3,2,1,0:T(8,128)(2,1)S(1)}, bf16[4,2,128,512]{3,2,1,0:T(8,128)(2,1)S(1)}, u32[]{:S(2)}, u32[]{:S(2)}) collective-permute-start(bf16[4,2,128,512]{3,2,1,0:T(8,128)(2,1)S(1)} %collective-permute-done.21.refs_8_.refs_9_), channel_id=1, source_target_pairs={{0,4},{4,0},{1,5},{5,1},{2,6},{6,2},{3,7},{7,3},{8,12},{12,8},{9,1... | collective-permute-start | bytes 3145736 | tf_op jit(solution)/shard_map/ppermute | solution.py:410
  99.0 2.6 %collective-permute-start.23 = (bf16[2,2,128,512]{3,2,1,0:T(8,128)(2,1)S(1)}, bf16[2,2,128,512]{3,2,1,0:T(8,128)(2,1)S(1)}, u32[]{:S(2)}, u32[]{:S(2)}) collective-permute-start(bf16[2,2,128,512]{3,2,1,0:T(8,128)(2,1)S(1)} %slice.87), channel_id=1, source_target_pairs={{0,32},{4,12},{8,40},{12,20},{16,48},{20,28},{24,56},{28,4},{32,64... | collective-permute-start | bytes 1572872 | tf_op jit(solution)/shard_map/ppermute | solution.py:379
  101.7 0.7 collective-permute-start.24
  102.5 0.8 collective-permute-start.13
  103.3 7.2 %collective-permute-done.23.refs_10_.refs_11_ = bf16[2,2,128,512]{3,2,1,0:T(8,128)(2,1)S(1)} collective-permute-done((bf16[2,2,128,512]{3,2,1,0:T(8,128)(2,1)S(1)}, bf16[2,2,128,512]{3,2,1,0:T(8,128)(2,1)S(1)}, u32[]{:S(2)}, u32[]{:S(2)}) %collective-permute-start.23) | collective-permute-done | bytes 524320 | tf_op jit(solution)/shard_map/ppermute | solution.py:379
  110.4 0.5 collective-permute-start.14
  111.0 1.9 collective-permute-start.28
  113.0 7.8 %collective-permute-done.14.refs_3_.refs_4_ = bf16[512,256]{1,0:T(8,128)(2,1)S(1)} collective-permute-done((bf16[512,256]{1,0:T(8,128)(2,1)S(1)}, bf16[512,256]{1,0:T(8,128)(2,1)S(1)}, u32[]{:S(2)}, u32[]{:S(2)}) %collective-permute-start.14) | collective-permute-done | bytes 262176 | tf_op jit(solution)/shard_map/ppermute | solution.py:407
  120.7 0.7 slice.83
  121.5 0.7 slice.84
  122.1 3.2 %collective-permute-start.15 = (bf16[256,256]{1,0:T(8,128)(2,1)}, bf16[256,256]{1,0:T(8,128)(2,1)S(1)}, u32[]{:S(2)}, u32[]{:S(2)}) collective-permute-start(bf16[256,256]{1,0:T(8,128)(2,1)} %slice.83), channel_id=1, source_target_pairs={{0,1},{1,2},{2,3},{3,0},{4,5},{5,6},{6,7},{7,4},{8,9},{9,10},{10,1... | collective-permute-start | bytes 393224 | tf_op jit(solution)/shard_map/ppermute | solution.py:407
  125.3 1.0 copy-done.43
  126.3 1.9 %collective-permute-done.15.refs_4_.refs_5_ = bf16[256,256]{1,0:T(8,128)(2,1)S(1)} collective-permute-done((bf16[256,256]{1,0:T(8,128)(2,1)}, bf16[256,256]{1,0:T(8,128)(2,1)S(1)}, u32[]{:S(2)}, u32[]{:S(2)}) %collective-permute-start.15) | collective-permute-done | bytes 131104 | tf_op jit(solution)/shard_map/ppermute | solution.py:407
  128.3 10.5 %collective-permute-done.16.refs_5_.refs_6_ = bf16[256,256]{1,0:T(8,128)(2,1)S(1)} collective-permute-done((bf16[256,256]{1,0:T(8,128)(2,1)}, bf16[256,256]{1,0:T(8,128)(2,1)S(1)}, u32[]{:S(2)}, u32[]{:S(2)}) %collective-permute-start.16) | collective-permute-done | bytes 131104 | tf_op jit(solution)/shard_map/ppermute | solution.py:407
  138.8 0.6 copy-done.30
  139.5 8.0 %token_parts.5 = (bf16[64,2048]{1,0:T(8,128)(2,1)}, bf16[64,2048]{1,0:T(8,128)(2,1)}) custom-call(s32[1]{0:T(128)} %bitcast.x_ref, s32[33]{0:T(128)} %copy-done.40, f32[1,2048]{1,0:T(1,128)} %bitcast.47, bf16[128,2048]{1,0:T(8,128)(2,1)} %copy-done.44, bf16[512,256]{1,0:T(8,128)(2,1)} %copy-done.18, bf16[512,256]{1,0:T(8,128)(2,1)} %copy-done.21, ...), custom_call_target="tpu_custom_call" | custom-call | flops 1610612736 | bytes 12582912 | tf_op jit(solution)/shard_map/token_parts/pallas_call | solution.py:338
  147.6 3.2 %collective-permute-start.33 = (bf16[64,2048]{1,0:T(8,128)(2,1)}, bf16[64,2048]{1,0:T(8,128)(2,1)S(1)}, u32[]{:S(2)}, u32[]{:S(2)}) collective-permute-start(bf16[64,2048]{1,0:T(8,128)(2,1)} %get-tuple-element.26), channel_id=1, source_target_pairs={{0,1},{1,2},{2,3},{3,0},{4,5},{5,6},{6,7},{7,4},{8,9},{9,10},{10,1... | collective-permute-start | bytes 786440 | tf_op jit(solution)/shard_map/ppermute | solution.py:407
  150.8 1.2 copy-done.5
  152.1 1.2 copy-done.7
  153.3 1.0 copy-done.12
  154.3 1.0 copy-done.15
  155.4 1.0 copy-done.17
  156.4 0.9 copy-done.19
  157.4 0.9 copy-done.22
  158.3 0.9 copy-done.25
  159.3 0.9 copy-done.28
  160.2 0.9 copy-done.31
  161.1 1.0 copy-done.34
  162.1 13.1 %token_parts.4 = (bf16[128,2048]{1,0:T(8,128)(2,1)S(1)}, bf16[128,2048]{1,0:T(8,128)(2,1)S(1)}) custom-call(s32[1]{0:T(128)} %bitcast.x_ref, s32[33]{0:T(128)S(1)} %copy-done.41, f32[1,2048]{1,0:T(1,128)S(1)} %bitcast.48, bf16[128,2048]{1,0:T(8,128)(2,1)S(1)} %copy-done.34, bf16[128,2048]{1,0:T(8,128)(2,1)} %collective-permute-done.31.refs_1_, ...), custom_call_target="tpu_custom_call" | custom-call | flops 3221225472 | bytes 12582912 | tf_op jit(solution)/shard_map/token_parts/pallas_call | solution.py:338
  175.5 3.3 %collective-permute-start.34 = (bf16[128,2048]{1,0:T(8,128)(2,1)S(1)}, bf16[128,2048]{1,0:T(8,128)(2,1)S(1)}, u32[]{:S(2)}, u32[]{:S(2)}) collective-permute-start(bf16[128,2048]{1,0:T(8,128)(2,1)S(1)} %add_convert_fusion.2), channel_id=1, source_target_pairs={{0,1},{1,2},{2,3},{3,0},{4,5},{5,6},{6,7},{7,4},{8,9},{9,10},{10,1... | collective-permute-start | bytes 1572872 | tf_op jit(solution)/shard_map/ppermute | solution.py:407
  178.8 13.6 %token_parts.3 = f32[128,2048]{1,0:T(8,128)S(1)} custom-call(s32[1]{0:T(128)} %bitcast.x_ref, s32[33]{0:T(128)S(1)} %copy-done.41, f32[1,2048]{1,0:T(1,128)S(1)} %bitcast.49, bf16[128,2048]{1,0:T(8,128)(2,1)} %refs_0_.1, bf16[512,256]{1,0:T(8,128)(2,1)S(1)} %copy-done.20, bf16[512,256]{1,0:T(8,128)(2,1)S(1)} %copy-done.23, bf16[512,256]{1,0:T(8,128)(2,1)S(1)} %copy-done.26, ...), custom_call_target="tpu_custom_call" | custom-call | flops 1610612736 | bytes 12582912 | tf_op jit(solution)/shard_map/token_parts/pallas_call | solution.py:338
  192.5 1.0 add_convert_fusion
  (165 shorter events, 2.6 us)
Async XLA Ops:
  2.4 1.8 collective-permute-start
  4.5 9.2 %collective-permute-start.2 = (bf16[2,8,128,128]{3,2,1,0:T(8,128)(2,1)S(1)}, bf16[2,8,128,128]{3,2,1,0:T(8,128)(2,1)S(1)}, u32[]{:S(2)}, u32[]{:S(2)}) collective-permute-start(bf16[2,8,128,128]{3,2,1,0:T(8,128)(2,1)S(1)} %get-tuple-element.31), channel_id=1, source_target_pairs={{0,8},{4,36},{8,16},{12,44},{16,24},{20,52},{24,0},{28,60},{32,40}... | collective-permute-start | bytes 1572872 | tf_op jit(solution)/shard_map/ppermute | solution.py:379
  5.8 12.3 %collective-permute-start.3 = (bf16[2,8,128,128]{3,2,1,0:T(8,128)(2,1)S(1)}, bf16[2,8,128,128]{3,2,1,0:T(8,128)(2,1)S(1)}, u32[]{:S(2)}, u32[]{:S(2)}) collective-permute-start(bf16[2,8,128,128]{3,2,1,0:T(8,128)(2,1)S(1)} %get-tuple-element.31), channel_id=1, source_target_pairs={{0,24},{4,100},{8,0},{12,108},{16,8},{20,116},{24,16},{28,124},{32... | collective-permute-start | bytes 1572872 | tf_op jit(solution)/shard_map/ppermute | solution.py:379
  13.7 12.5 %collective-permute-start.4 = (bf16[2,8,128,128]{3,2,1,0:T(8,128)(2,1)S(1)}, bf16[2,8,128,128]{3,2,1,0:T(8,128)(2,1)S(1)}, u32[]{:S(2)}, u32[]{:S(2)}) collective-permute-start(bf16[2,8,128,128]{3,2,1,0:T(8,128)(2,1)S(1)} %collective-permute-done.2), channel_id=1, source_target_pairs={{0,8},{4,36},{8,16},{12,44},{16,24},{20,52},{24,0},{28,60},{32,40}... | collective-permute-start | bytes 1572872 | tf_op jit(solution)/shard_map/ppermute | solution.py:379
  15.1 16.5 %collective-permute-start.17 = (bf16[2,64,512]{2,1,0:T(8,128)(2,1)S(1)}, bf16[2,64,512]{2,1,0:T(8,128)(2,1)S(1)}, u32[]{:S(2)}, u32[]{:S(2)}) collective-permute-start(bf16[2,64,512]{2,1,0:T(8,128)(2,1)S(1)} %broadcast_select_fusion.6), channel_id=1, source_target_pairs={{0,4},{4,0},{1,5},{5,1},{2,6},{6,2},{3,7},{7,3},{8,12},{12,8},{9,1... | collective-permute-start | bytes 393224 | tf_op jit(solution)/shard_map/ppermute | solution.py:410
  16.3 31.3 %collective-permute-start.5 = (bf16[2,2,8,128,128]{4,3,2,1,0:T(8,128)(2,1)}, bf16[2,2,8,128,128]{4,3,2,1,0:T(8,128)(2,1)}, u32[]{:S(2)}, u32[]{:S(2)}) collective-permute-start(bf16[2,2,8,128,128]{4,3,2,1,0:T(8,128)(2,1)} %pad_maximum_fusion), channel_id=1, source_target_pairs={{0,32},{4,12},{8,40},{12,20},{16,48},{20,28},{24,56},{28,4},{32,64... | collective-permute-start | bytes 3145736 | tf_op jit(solution)/shard_map/ppermute | solution.py:379
  18.2 13.4 %copy-start.35 = (bf16[2,8,128,128]{3,2,1,0:T(8,128)(2,1)}, bf16[2,8,128,128]{3,2,1,0:T(8,128)(2,1)S(1)}, u32[]{:S(2)}) copy-start(bf16[2,8,128,128]{3,2,1,0:T(8,128)(2,1)S(1)} %collective-permute-done.3) | copy-start | bytes 1572868
  27.5 13.8 %copy-start.54 = (s32[16]{0:T(128)S(1)}, s32[16]{0:T(128)}, u32[]{:S(2)}) copy-start(s32[16]{0:T(128)} %constant.62.clone) | copy-start | bytes 196
  27.5 13.8 %copy-start.55 = (s32[16]{0:T(128)S(1)}, s32[16]{0:T(128)}, u32[]{:S(2)}) copy-start(s32[16]{0:T(128)} %constant.61.clone) | copy-start | bytes 196
  27.5 19.5 %copy-start.52 = (f32[2]{0:T(128)S(1)}, f32[2]{0:T(128)}, u32[]{:S(2)}) copy-start(f32[2]{0:T(128)} %param.16) | copy-start | bytes 28
  27.5 25.0 %collective-permute-start.8 = (bf16[2,2,8,128,128]{4,3,2,1,0:T(8,128)(2,1)}, bf16[2,2,8,128,128]{4,3,2,1,0:T(8,128)(2,1)}, u32[]{:S(2)}, u32[]{:S(2)}) collective-permute-start(bf16[2,2,8,128,128]{4,3,2,1,0:T(8,128)(2,1)} %pad_maximum_fusion.1), channel_id=1, source_target_pairs={{0,96},{4,28},{8,104},{12,4},{16,112},{20,12},{24,120},{28,20},{32... | collective-permute-start | bytes 3145736 | tf_op jit(solution)/shard_map/ppermute | solution.py:379
  31.6 21.4 %copy-start.53 = (pred[128]{0:T(512)(128)(4,1)S(1)}, pred[128]{0:T(512)(128)(4,1)}, u32[]{:S(2)}) copy-start(pred[128]{0:T(512)(128)(4,1)} %constant.58.clone.1) | copy-start | bytes 388
  31.7 6.7 %collective-permute-start.18 = (bf16[2,128,512]{2,1,0:T(8,128)(2,1)S(1)}, bf16[2,128,512]{2,1,0:T(8,128)(2,1)S(1)}, u32[]{:S(2)}, u32[]{:S(2)}) collective-permute-start(bf16[2,128,512]{2,1,0:T(8,128)(2,1)S(1)} %get-tuple-element.36), channel_id=1, source_target_pairs={{0,8},{4,36},{8,16},{12,44},{16,24},{20,52},{24,0},{28,60},{32,40}... | collective-permute-start | bytes 786440 | tf_op jit(solution)/shard_map/ppermute | solution.py:379
  32.9 10.8 %collective-permute-start.19 = (bf16[2,128,512]{2,1,0:T(8,128)(2,1)S(1)}, bf16[2,128,512]{2,1,0:T(8,128)(2,1)S(1)}, u32[]{:S(2)}, u32[]{:S(2)}) collective-permute-start(bf16[2,128,512]{2,1,0:T(8,128)(2,1)S(1)} %get-tuple-element.36), channel_id=1, source_target_pairs={{0,24},{4,100},{8,0},{12,108},{16,8},{20,116},{24,16},{28,124},{32... | collective-permute-start | bytes 786440 | tf_op jit(solution)/shard_map/ppermute | solution.py:379
  33.8 13.8 %collective-permute-start.1 = (bf16[4,128,128]{2,1,0:T(8,128)(2,1)S(1)}, bf16[4,128,128]{2,1,0:T(8,128)(2,1)S(1)}, u32[]{:S(2)}, u32[]{:S(2)}) collective-permute-start(bf16[4,128,128]{2,1,0:T(8,128)(2,1)S(1)} %slice.79), channel_id=1, source_target_pairs={{0,120},{8,112},{16,104},{24,96},{32,88},{40,80},{48,72},{56,64},{... | collective-permute-start | bytes 393224 | tf_op jit(solution)/shard_map/ppermute | solution.py:428
  38.4 14.7 %copy-start.48 = (bf16[2,128,512]{2,1,0:T(8,128)(2,1)}, bf16[2,128,512]{2,1,0:T(8,128)(2,1)S(1)}, u32[]{:S(2)}) copy-start(bf16[2,128,512]{2,1,0:T(8,128)(2,1)S(1)} %collective-permute-done.18) | copy-start | bytes 786436
  38.4 27.2 %collective-permute-start.6 = (bf16[2,2,8,128,128]{4,3,2,1,0:T(8,128)(2,1)}, bf16[2,2,8,128,128]{4,3,2,1,0:T(8,128)(2,1)}, u32[]{:S(2)}, u32[]{:S(2)}) collective-permute-start(bf16[2,2,8,128,128]{4,3,2,1,0:T(8,128)(2,1)} %pad_maximum_fusion), channel_id=1, source_target_pairs={{0,96},{4,28},{8,104},{12,4},{16,112},{20,12},{24,120},{28,20},{32... | collective-permute-start | bytes 3145736 | tf_op jit(solution)/shard_map/ppermute | solution.py:379
  43.7 7.9 %collective-permute-start.20 = (bf16[2,128,512]{2,1,0:T(8,128)(2,1)S(1)}, bf16[2,128,512]{2,1,0:T(8,128)(2,1)S(1)}, u32[]{:S(2)}, u32[]{:S(2)}) collective-permute-start(bf16[2,128,512]{2,1,0:T(8,128)(2,1)S(1)} %collective-permute-done.18), channel_id=1, source_target_pairs={{0,8},{4,36},{8,16},{12,44},{16,24},{20,52},{24,0},{28,60},{32,40}... | collective-permute-start | bytes 786440 | tf_op jit(solution)/shard_map/ppermute | solution.py:379
  47.6 32.3 %collective-permute-start.7 = (bf16[2,2,8,128,128]{4,3,2,1,0:T(8,128)(2,1)}, bf16[2,2,8,128,128]{4,3,2,1,0:T(8,128)(2,1)}, u32[]{:S(2)}, u32[]{:S(2)}) collective-permute-start(bf16[2,2,8,128,128]{4,3,2,1,0:T(8,128)(2,1)} %pad_maximum_fusion.1), channel_id=1, source_target_pairs={{0,32},{4,12},{8,40},{12,20},{16,48},{20,28},{24,56},{28,4},{32,64... | collective-permute-start | bytes 3145736 | tf_op jit(solution)/shard_map/ppermute | solution.py:379
  47.6 33.9 %collective-permute-start.9 = (bf16[2,2,8,128,128]{4,3,2,1,0:T(8,128)(2,1)}, bf16[2,2,8,128,128]{4,3,2,1,0:T(8,128)(2,1)}, u32[]{:S(2)}, u32[]{:S(2)}) collective-permute-start(bf16[2,2,8,128,128]{4,3,2,1,0:T(8,128)(2,1)} %collective-permute-done.5.refs_5_), channel_id=1, source_target_pairs={{0,32},{4,12},{8,40},{12,20},{16,48},{20,28},{24,56},{28,4},{32,64... | collective-permute-start | bytes 3145736 | tf_op jit(solution)/shard_map/ppermute | solution.py:379
  47.7 39.5 %copy-start.40 = (s32[33]{0:T(128)}, s32[33]{0:T(128)S(1)}, u32[]{:S(2)}) copy-start(s32[33]{0:T(128)S(1)} %pad_add_fusion.ids_ref.chips_ref) | copy-start | bytes 400
  51.7 14.0 %collective-permute-start.30 = (bf16[128,2048]{1,0:T(8,128)(2,1)}, bf16[128,2048]{1,0:T(8,128)(2,1)S(1)}, u32[]{:S(2)}, u32[]{:S(2)}) collective-permute-start(bf16[128,2048]{1,0:T(8,128)(2,1)} %refs_0_.1), channel_id=1, source_target_pairs={{0,1},{1,2},{2,3},{3,0},{4,5},{5,6},{6,7},{7,4},{8,9},{9,10},{10,1... | collective-permute-start | bytes 1572872 | tf_op jit(solution)/shard_map/ppermute | solution.py:407
  52.5 34.7 %collective-permute-start.10 = (bf16[2,2,8,128,128]{4,3,2,1,0:T(8,128)(2,1)}, bf16[2,2,8,128,128]{4,3,2,1,0:T(8,128)(2,1)S(1)}, u32[]{:S(2)}, u32[]{:S(2)}) collective-permute-start(bf16[2,2,8,128,128]{4,3,2,1,0:T(8,128)(2,1)} %collective-permute-done.8.refs_3_), channel_id=1, source_target_pairs={{0,96},{4,28},{8,104},{12,4},{16,112},{20,12},{24,120},{28,20},{32... | collective-permute-start | bytes 3145736 | tf_op jit(solution)/shard_map/ppermute | solution.py:379
  57.7 11.2 %copy-start.36 = (bf16[2,8,128,128]{3,2,1,0:T(8,128)(2,1)S(1)}, bf16[2,8,128,128]{3,2,1,0:T(8,128)(2,1)}, u32[]{:S(2)}) copy-start(bf16[2,8,128,128]{3,2,1,0:T(8,128)(2,1)} %copy-done.35) | copy-start | bytes 1572868
  57.7 11.2 %copy-start.38 = (bf16[2,8,128,128]{3,2,1,0:T(8,128)(2,1)S(1)}, bf16[2,8,128,128]{3,2,1,0:T(8,128)(2,1)}, u32[]{:S(2)}) copy-start(bf16[2,8,128,128]{3,2,1,0:T(8,128)(2,1)} %copy-done.37) | copy-start | bytes 1572868
  57.9 23.6 %copy-start = (bf16[4,2,128,512]{3,2,1,0:T(8,128)(2,1)}, bf16[4,2,128,512]{3,2,1,0:T(8,128)(2,1)S(1)}, u32[]{:S(2)}) copy-start(bf16[4,2,128,512]{3,2,1,0:T(8,128)(2,1)S(1)} %pad_maximum_fusion.2.refs_7_.refs_8_) | copy-start | bytes 3145732
  65.6 14.2 %copy-start.33 = (bf16[128,2048]{1,0:T(8,128)(2,1)}, bf16[128,2048]{1,0:T(8,128)(2,1)S(1)}, u32[]{:S(2)}) copy-start(bf16[128,2048]{1,0:T(8,128)(2,1)S(1)} %collective-permute-done.30.refs_0_) | copy-start | bytes 1572868
  65.6 29.9 %collective-permute-start.21 = (bf16[4,2,128,512]{3,2,1,0:T(8,128)(2,1)S(1)}, bf16[4,2,128,512]{3,2,1,0:T(8,128)(2,1)S(1)}, u32[]{:S(2)}, u32[]{:S(2)}) collective-permute-start(bf16[4,2,128,512]{3,2,1,0:T(8,128)(2,1)S(1)} %pad_maximum_fusion.2.refs_7_.refs_8_), channel_id=1, source_target_pairs={{0,32},{4,12},{8,40},{12,20},{16,48},{20,28},{24,56},{28,4},{32,64... | collective-permute-start | bytes 3145736 | tf_op jit(solution)/shard_map/ppermute | solution.py:379
  65.6 33.2 %collective-permute-start.22 = (bf16[4,2,128,512]{3,2,1,0:T(8,128)(2,1)S(1)}, bf16[4,2,128,512]{3,2,1,0:T(8,128)(2,1)S(1)}, u32[]{:S(2)}, u32[]{:S(2)}) collective-permute-start(bf16[4,2,128,512]{3,2,1,0:T(8,128)(2,1)S(1)} %pad_maximum_fusion.2.refs_7_.refs_8_), channel_id=1, source_target_pairs={{0,96},{4,28},{8,104},{12,4},{16,112},{20,12},{24,120},{28,20},{32... | collective-permute-start | bytes 3145736 | tf_op jit(solution)/shard_map/ppermute | solution.py:379
  79.9 15.0 %collective-permute-start.32 = (bf16[128,2048]{1,0:T(8,128)(2,1)S(1)}, bf16[128,2048]{1,0:T(8,128)(2,1)S(1)}, u32[]{:S(2)}, u32[]{:S(2)}) collective-permute-start(bf16[128,2048]{1,0:T(8,128)(2,1)S(1)} %collective-permute-done.30.refs_0_), channel_id=1, source_target_pairs={{0,1},{1,2},{2,3},{3,0},{4,5},{5,6},{6,7},{7,4},{8,9},{9,10},{10,1... | collective-permute-start | bytes 1572872 | tf_op jit(solution)/shard_map/ppermute | solution.py:407
  81.4 21.0 %collective-permute-start.25 = (bf16[4,2,128,512]{3,2,1,0:T(8,128)(2,1)S(1)}, bf16[4,2,128,512]{3,2,1,0:T(8,128)(2,1)S(1)}, u32[]{:S(2)}, u32[]{:S(2)}) collective-permute-start(bf16[4,2,128,512]{3,2,1,0:T(8,128)(2,1)S(1)} %pad_maximum_fusion.2.refs_7_.refs_8_), channel_id=1, source_target_pairs={{0,4},{4,0},{1,5},{5,1},{2,6},{6,2},{3,7},{7,3},{8,12},{12,8},{9,1... | collective-permute-start | bytes 3145736 | tf_op jit(solution)/shard_map/ppermute | solution.py:410
  94.2 4.7 %collective-permute-start.11 = (bf16[512,128]{1,0:T(8,128)(2,1)S(1)}, bf16[512,128]{1,0:T(8,128)(2,1)S(1)}, u32[]{:S(2)}, u32[]{:S(2)}) collective-permute-start(bf16[512,128]{1,0:T(8,128)(2,1)S(1)} %broadcast_select_fusion.10), channel_id=1, source_target_pairs={{4,0},{12,8},{20,16},{28,24},{36,32},{44,40},{52,48},{60,56},{68,6... | collective-permute-start | bytes 393224 | tf_op jit(solution)/shard_map/ppermute | solution.py:501
  94.9 6.7 %collective-permute-start.12 = (bf16[512,128]{1,0:T(8,128)(2,1)S(1)}, bf16[512,128]{1,0:T(8,128)(2,1)S(1)}, u32[]{:S(2)}, u32[]{:S(2)}) collective-permute-start(bf16[512,128]{1,0:T(8,128)(2,1)S(1)} %get-tuple-element.24), channel_id=1, source_target_pairs={{4,124},{12,116},{20,108},{28,100},{36,92},{44,84},{52,76},{60,68}... | collective-permute-start | bytes 393224 | tf_op jit(solution)/shard_map/ppermute | solution.py:500
  95.6 26.5 %collective-permute-start.26 = (bf16[4,2,128,512]{3,2,1,0:T(8,128)(2,1)S(1)}, bf16[4,2,128,512]{3,2,1,0:T(8,128)(2,1)S(1)}, u32[]{:S(2)}, u32[]{:S(2)}) collective-permute-start(bf16[4,2,128,512]{3,2,1,0:T(8,128)(2,1)S(1)} %collective-permute-done.21.refs_8_.refs_9_), channel_id=1, source_target_pairs={{0,4},{4,0},{1,5},{5,1},{2,6},{6,2},{3,7},{7,3},{8,12},{12,8},{9,1... | collective-permute-start | bytes 3145736 | tf_op jit(solution)/shard_map/ppermute | solution.py:410
  98.8 26.5 %collective-permute-start.27 = (bf16[4,2,128,512]{3,2,1,0:T(8,128)(2,1)S(1)}, bf16[4,2,128,512]{3,2,1,0:T(8,128)(2,1)S(1)}, u32[]{:S(2)}, u32[]{:S(2)}) collective-permute-start(bf16[4,2,128,512]{3,2,1,0:T(8,128)(2,1)S(1)} %collective-permute-done.22.refs_9_.refs_10_), channel_id=1, source_target_pairs={{0,4},{4,0},{1,5},{5,1},{2,6},{6,2},{3,7},{7,3},{8,12},{12,8},{9,1... | collective-permute-start | bytes 3145736 | tf_op jit(solution)/shard_map/ppermute | solution.py:410
  99.0 11.5 %collective-permute-start.23 = (bf16[2,2,128,512]{3,2,1,0:T(8,128)(2,1)S(1)}, bf16[2,2,128,512]{3,2,1,0:T(8,128)(2,1)S(1)}, u32[]{:S(2)}, u32[]{:S(2)}) collective-permute-start(bf16[2,2,128,512]{3,2,1,0:T(8,128)(2,1)S(1)} %slice.87), channel_id=1, source_target_pairs={{0,32},{4,12},{8,40},{12,20},{16,48},{20,28},{24,56},{28,4},{32,64... | collective-permute-start | bytes 1572872 | tf_op jit(solution)/shard_map/ppermute | solution.py:379
  101.7 9.4 %collective-permute-start.24 = (bf16[2,2,128,512]{3,2,1,0:T(8,128)(2,1)S(1)}, bf16[2,2,128,512]{3,2,1,0:T(8,128)(2,1)}, u32[]{:S(2)}, u32[]{:S(2)}) collective-permute-start(bf16[2,2,128,512]{3,2,1,0:T(8,128)(2,1)S(1)} %slice.88), channel_id=1, source_target_pairs={{0,96},{4,28},{8,104},{12,4},{16,112},{20,12},{24,120},{28,20},{32... | collective-permute-start | bytes 1572872 | tf_op jit(solution)/shard_map/ppermute | solution.py:379
  102.5 37.0 %copy-start.18 = (bf16[512,256]{1,0:T(8,128)(2,1)}, bf16[512,256]{1,0:T(8,128)(2,1)S(1)}, u32[]{:S(2)}) copy-start(bf16[512,256]{1,0:T(8,128)(2,1)S(1)} %pad_maximum_fusion.7.refs_1_.refs_2_) | copy-start | bytes 786436
  102.5 22.8 %copy-start.6 = (bf16[4,2,128,512]{3,2,1,0:T(8,128)(2,1)}, bf16[4,2,128,512]{3,2,1,0:T(8,128)(2,1)S(1)}, u32[]{:S(2)}) copy-start(bf16[4,2,128,512]{3,2,1,0:T(8,128)(2,1)S(1)} %collective-permute-done.25.refs_12_.refs_13_) | copy-start | bytes 3145732
  102.5 10.4 %collective-permute-start.13 = (bf16[512,256]{1,0:T(8,128)(2,1)S(1)}, bf16[512,256]{1,0:T(8,128)(2,1)S(1)}, u32[]{:S(2)}, u32[]{:S(2)}) collective-permute-start(bf16[512,256]{1,0:T(8,128)(2,1)S(1)} %pad_maximum_fusion.7.refs_1_.refs_2_), channel_id=1, source_target_pairs={{0,1},{1,2},{2,3},{3,0},{4,5},{5,6},{6,7},{7,4},{8,9},{9,10},{10,1... | collective-permute-start | bytes 786440 | tf_op jit(solution)/shard_map/ppermute | solution.py:407
  110.4 29.0 %copy-start.11 = (bf16[2,2,128,512]{3,2,1,0:T(8,128)(2,1)}, bf16[2,2,128,512]{3,2,1,0:T(8,128)(2,1)S(1)}, u32[]{:S(2)}) copy-start(bf16[2,2,128,512]{3,2,1,0:T(8,128)(2,1)S(1)} %collective-permute-done.23.refs_10_.refs_11_) | copy-start | bytes 1572868
  110.4 10.3 %collective-permute-start.14 = (bf16[512,256]{1,0:T(8,128)(2,1)S(1)}, bf16[512,256]{1,0:T(8,128)(2,1)S(1)}, u32[]{:S(2)}, u32[]{:S(2)}) collective-permute-start(bf16[512,256]{1,0:T(8,128)(2,1)S(1)} %pad_maximum_fusion.7.refs_1_.refs_2_), channel_id=1, source_target_pairs={{0,3},{1,0},{2,1},{3,2},{4,7},{5,4},{6,5},{7,6},{8,11},{9,8},{10,9... | collective-permute-start | bytes 786440 | tf_op jit(solution)/shard_map/ppermute | solution.py:407
  111.0 15.3 %collective-permute-start.28 = (bf16[2,2,128,512]{3,2,1,0:T(8,128)(2,1)S(1)}, bf16[2,2,128,512]{3,2,1,0:T(8,128)(2,1)S(1)}, u32[]{:S(2)}, u32[]{:S(2)}) collective-permute-start(bf16[2,2,128,512]{3,2,1,0:T(8,128)(2,1)S(1)} %collective-permute-done.23.refs_10_.refs_11_), channel_id=1, source_target_pairs={{0,4},{4,0},{1,5},{5,1},{2,6},{6,2},{3,7},{7,3},{8,12},{12,8},{9,1... | collective-permute-start | bytes 1572872 | tf_op jit(solution)/shard_map/ppermute | solution.py:410
  112.9 25.9 %copy-start.21 = (bf16[512,256]{1,0:T(8,128)(2,1)}, bf16[512,256]{1,0:T(8,128)(2,1)S(1)}, u32[]{:S(2)}) copy-start(bf16[512,256]{1,0:T(8,128)(2,1)S(1)} %collective-permute-done.13.refs_2_.refs_3_) | copy-start | bytes 786436
  112.9 13.4 %collective-permute-start.29 = (bf16[2,2,128,512]{3,2,1,0:T(8,128)(2,1)}, bf16[2,2,128,512]{3,2,1,0:T(8,128)(2,1)S(1)}, u32[]{:S(2)}, u32[]{:S(2)}) collective-permute-start(bf16[2,2,128,512]{3,2,1,0:T(8,128)(2,1)} %collective-permute-done.24.refs_11_.refs_12_), channel_id=1, source_target_pairs={{0,4},{4,0},{1,5},{5,1},{2,6},{6,2},{3,7},{7,3},{8,12},{12,8},{9,1... | collective-permute-start | bytes 1572872 | tf_op jit(solution)/shard_map/ppermute | solution.py:410
  120.7 30.1 %collective-permute-start.31 = (bf16[128,2048]{1,0:T(8,128)(2,1)}, bf16[128,2048]{1,0:T(8,128)(2,1)}, u32[]{:S(2)}, u32[]{:S(2)}) collective-permute-start(bf16[128,2048]{1,0:T(8,128)(2,1)} %refs_0_.1), channel_id=1, source_target_pairs={{0,3},{1,0},{2,1},{3,2},{4,7},{5,4},{6,5},{7,6},{8,11},{9,8},{10,9... | collective-permute-start | bytes 1572872 | tf_op jit(solution)/shard_map/ppermute | solution.py:407
  122.1 6.1 %collective-permute-start.15 = (bf16[256,256]{1,0:T(8,128)(2,1)}, bf16[256,256]{1,0:T(8,128)(2,1)S(1)}, u32[]{:S(2)}, u32[]{:S(2)}) collective-permute-start(bf16[256,256]{1,0:T(8,128)(2,1)} %slice.83), channel_id=1, source_target_pairs={{0,1},{1,2},{2,3},{3,0},{4,5},{5,6},{6,7},{7,4},{8,9},{9,10},{10,1... | collective-permute-start | bytes 393224 | tf_op jit(solution)/shard_map/ppermute | solution.py:407
  126.3 12.5 %collective-permute-start.16 = (bf16[256,256]{1,0:T(8,128)(2,1)}, bf16[256,256]{1,0:T(8,128)(2,1)S(1)}, u32[]{:S(2)}, u32[]{:S(2)}) collective-permute-start(bf16[256,256]{1,0:T(8,128)(2,1)} %slice.84), channel_id=1, source_target_pairs={{0,3},{1,0},{2,1},{3,2},{4,7},{5,4},{6,5},{7,6},{8,11},{9,8},{10,9... | collective-permute-start | bytes 393224 | tf_op jit(solution)/shard_map/ppermute | solution.py:407
  126.3 12.5 %copy-start.14 = (bf16[2,2,128,512]{3,2,1,0:T(8,128)(2,1)}, bf16[2,2,128,512]{3,2,1,0:T(8,128)(2,1)S(1)}, u32[]{:S(2)}) copy-start(bf16[2,2,128,512]{3,2,1,0:T(8,128)(2,1)S(1)} %collective-permute-done.28.refs_15_.refs_16_) | copy-start | bytes 1572868
  126.3 12.5 %copy-start.16 = (bf16[2,2,128,512]{3,2,1,0:T(8,128)(2,1)}, bf16[2,2,128,512]{3,2,1,0:T(8,128)(2,1)S(1)}, u32[]{:S(2)}) copy-start(bf16[2,2,128,512]{3,2,1,0:T(8,128)(2,1)S(1)} %collective-permute-done.29.refs_16_.refs_17_) | copy-start | bytes 1572868
  128.3 11.2 %copy-start.27 = (bf16[256,256]{1,0:T(8,128)(2,1)}, bf16[256,256]{1,0:T(8,128)(2,1)S(1)}, u32[]{:S(2)}) copy-start(bf16[256,256]{1,0:T(8,128)(2,1)S(1)} %collective-permute-done.15.refs_4_.refs_5_) | copy-start | bytes 393220
  139.5 11.3 %copy-start.1 = (bf16[4,2,128,512]{3,2,1,0:T(8,128)(2,1)S(1)}, bf16[4,2,128,512]{3,2,1,0:T(8,128)(2,1)}, u32[]{:S(2)}) copy-start(bf16[4,2,128,512]{3,2,1,0:T(8,128)(2,1)} %copy-done) | copy-start | bytes 3145732
  139.5 11.3 %copy-start.3 = (bf16[4,2,128,512]{3,2,1,0:T(8,128)(2,1)S(1)}, bf16[4,2,128,512]{3,2,1,0:T(8,128)(2,1)}, u32[]{:S(2)}) copy-start(bf16[4,2,128,512]{3,2,1,0:T(8,128)(2,1)} %copy-done.2) | copy-start | bytes 3145732
  139.5 11.3 %copy-start.39 = (f32[2048]{0:T(1024)S(1)}, f32[2048]{0:T(1024)}, u32[]{:S(2)}) copy-start(f32[2048]{0:T(1024)} %param.19) | copy-start | bytes 24580
  139.5 11.3 %copy-start.41 = (s32[33]{0:T(128)S(1)}, s32[33]{0:T(128)}, u32[]{:S(2)}) copy-start(s32[33]{0:T(128)} %copy-done.40) | copy-start | bytes 400
  147.5 27.7 %collective-permute-start.35 = (bf16[64,2048]{1,0:T(8,128)(2,1)}, bf16[64,2048]{1,0:T(8,128)(2,1)S(1)}, u32[]{:S(2)}, u32[]{:S(2)}) collective-permute-start(bf16[64,2048]{1,0:T(8,128)(2,1)} %get-tuple-element.28), channel_id=1, source_target_pairs={{0,3},{1,0},{2,1},{3,2},{4,7},{5,4},{6,5},{7,6},{8,11},{9,8},{10,9... | collective-permute-start | bytes 786440 | tf_op jit(solution)/shard_map/ppermute | solution.py:407
  147.6 27.8 %collective-permute-start.33 = (bf16[64,2048]{1,0:T(8,128)(2,1)}, bf16[64,2048]{1,0:T(8,128)(2,1)S(1)}, u32[]{:S(2)}, u32[]{:S(2)}) collective-permute-start(bf16[64,2048]{1,0:T(8,128)(2,1)} %get-tuple-element.26), channel_id=1, source_target_pairs={{0,1},{1,2},{2,3},{3,0},{4,5},{5,6},{6,7},{7,4},{8,9},{9,10},{10,1... | collective-permute-start | bytes 786440 | tf_op jit(solution)/shard_map/ppermute | solution.py:407
  162.1 16.7 %copy-start.20 = (bf16[512,256]{1,0:T(8,128)(2,1)S(1)}, bf16[512,256]{1,0:T(8,128)(2,1)}, u32[]{:S(2)}) copy-start(bf16[512,256]{1,0:T(8,128)(2,1)} %copy-done.18) | copy-start | bytes 786436
  162.1 16.7 %copy-start.23 = (bf16[512,256]{1,0:T(8,128)(2,1)S(1)}, bf16[512,256]{1,0:T(8,128)(2,1)}, u32[]{:S(2)}) copy-start(bf16[512,256]{1,0:T(8,128)(2,1)} %copy-done.21) | copy-start | bytes 786436
  162.1 16.7 %copy-start.26 = (bf16[512,256]{1,0:T(8,128)(2,1)S(1)}, bf16[512,256]{1,0:T(8,128)(2,1)}, u32[]{:S(2)}) copy-start(bf16[512,256]{1,0:T(8,128)(2,1)} %copy-done.24) | copy-start | bytes 786436
  162.1 16.7 %copy-start.29 = (bf16[256,256]{1,0:T(8,128)(2,1)S(1)}, bf16[256,256]{1,0:T(8,128)(2,1)}, u32[]{:S(2)}) copy-start(bf16[256,256]{1,0:T(8,128)(2,1)} %copy-done.27) | copy-start | bytes 393220
  162.1 16.7 %copy-start.32 = (bf16[256,256]{1,0:T(8,128)(2,1)S(1)}, bf16[256,256]{1,0:T(8,128)(2,1)}, u32[]{:S(2)}) copy-start(bf16[256,256]{1,0:T(8,128)(2,1)} %copy-done.30) | copy-start | bytes 393220
  175.3 17.1 %collective-permute-start.36 = (bf16[128,2048]{1,0:T(8,128)(2,1)S(1)}, bf16[128,2048]{1,0:T(8,128)(2,1)S(1)}, u32[]{:S(2)}, u32[]{:S(2)}) collective-permute-start(bf16[128,2048]{1,0:T(8,128)(2,1)S(1)} %add_convert_fusion.1), channel_id=1, source_target_pairs={{0,3},{1,0},{2,1},{3,2},{4,7},{5,4},{6,5},{7,6},{8,11},{9,8},{10,9... | collective-permute-start | bytes 1572872 | tf_op jit(solution)/shard_map/ppermute | solution.py:407
  175.5 17.0 %collective-permute-start.34 = (bf16[128,2048]{1,0:T(8,128)(2,1)S(1)}, bf16[128,2048]{1,0:T(8,128)(2,1)S(1)}, u32[]{:S(2)}, u32[]{:S(2)}) collective-permute-start(bf16[128,2048]{1,0:T(8,128)(2,1)S(1)} %add_convert_fusion.2), channel_id=1, source_target_pairs={{0,1},{1,2},{2,3},{3,0},{4,5},{5,6},{6,7},{7,4},{8,9},{9,10},{10,1... | collective-permute-start | bytes 1572872 | tf_op jit(solution)/shard_map/ppermute | solution.py:407
  (29 other events, 100.7 us)
